TPU v7x, 512 devices: a whole 4x8x8 slice. The times are simulated.
512 devices in a mesh: sp: 64 (over z, y), fs: 4 (over x), tp: 2 (over core).
Axes of the slice: x: 4, y: 8, z: 8, core: 2. Of those that a mesh axis runs over, the one named last changes fastest.
Arguments:
- tokens: bfloat16 [8192, 2048], P(('sp', 'fs', 'tp')), may hold values from -16 to 16
- in_gain: float32 [2048], replicated, may hold values from 0.1 to 1.9
- ret_query: bfloat16 [2048, 1024], P(None, ('fs', 'tp')), may hold values from -0.125 to 0.125
- ret_key: bfloat16 [2048, 1024], P(None, ('fs', 'tp')), may hold values from -0.125 to 0.125
- ret_value: bfloat16 [2048, 1024], P(None, ('fs', 'tp')), may hold values from -0.125 to 0.125
- decay_log: float32 [8, 8192], P(('fs', 'tp'), 'sp'), may hold values from -1 to 0
- init_state: bfloat16 [8, 128, 128], P(('fs', 'tp')), may hold values from -24 to 24
- ret_gain: float32 [1024], P(('fs', 'tp')), may hold values from 0.1 to 1.9
- diff_query: bfloat16 [2, 2048, 512], P(None, None, ('fs', 'tp')), may hold values from -1 to 1
- diff_key: bfloat16 [2, 2048, 512], P(None, None, ('fs', 'tp')), may hold values from -1 to 1
- diff_value: bfloat16 [2048, 1024], P(None, ('fs', 'tp')), may hold values from -0.125 to 0.125
- diff_lambda: float32 [8], P(('fs', 'tp')), may hold values from 0.3 to 0.8
- diff_gain: float32 [1024], P(('fs', 'tp')), may hold values from 0.1 to 1.9
- out_weight: bfloat16 [2, 1024, 2048], P(None, ('fs', 'tp'), 'sp'), may hold values from -0.125 to 0.125
Outputs:
- mixed: bfloat16 [8192, 2048], P(('sp', 'fs', 'tp'))
All inputs are finite; a program needn't handle non-finite values.
Results may differ from a plain program's by a relative error of at most 0.017.
Values may be sent and summed in bfloat16 or wider, within the bound.
A program may use at most 64 MiB of HBM per device.

v0:
```python
import jax
import jax.numpy as jnp
from jax import lax
from jax.sharding import Mesh
from jax.sharding import PartitionSpec as P

RBLOCK = 128
SP = ("sp_0", "sp_1")
SP_FS_TP = ("sp_0", "sp_1", "fs", "tp")


EPS = 1e-06
HUGE = 1e30
UPPER_LIMIT = lax.Precision.HIGHEST


def from_everyone(x, axis):
    size = lax.axis_size(axis)
    return lax.all_to_all(jnp.broadcast_to(x[None], (size, *x.shape)), axis, 0, 0, tiled=True)


def in_order(pieces, dim):
    lengths = list(pieces.shape[1:])
    lengths[dim] *= pieces.shape[0]
    return jnp.moveaxis(pieces, 0, dim).reshape(lengths)


def gathered_copies(x, axis, dim):
    pieces = from_everyone(x, axis)
    return in_order(pieces, dim)


def filled_with(x, identity):
    return jnp.broadcast_to(jnp.asarray(identity, x.dtype), x.shape)


def prefix_by_axis(x, axes, combine, identity):
    before = start = filled_with(x, identity)
    total = x
    for axis in reversed(axes):
        size, position = (lax.axis_size(axis), lax.axis_index(axis))
        pieces = lax.all_gather(total.astype(jnp.bfloat16), axis)
        inside, total = (start, start)
        for k in range(size):
            passed = k < position
            total = combine(total, pieces[k].astype(x.dtype))
            inside = jnp.where(passed, total, inside)
        before = combine(inside, before)
    return before


def cut_along(x, dim, size):
    lengths = x.shape
    pieces = x.reshape(*lengths[:dim], size, lengths[dim] // size, *lengths[dim + 1 :])
    return jnp.moveaxis(pieces, dim, 0)


def sum_at_owner(x, axis, dim):
    size = lax.axis_size(axis)
    pieces = lax.all_to_all(cut_along(x, dim, size), axis, 0, 0, tiled=True)
    return jnp.sum(pieces.astype(jnp.float32), axis=0)


def norm_rows(rows, gain):
    widened = rows.astype(jnp.float32)
    fading_multiplier = lax.rsqrt(jnp.mean(widened * widened, axis=-1, keepdims=True) + EPS)
    return (widened * fading_multiplier * gain).astype(jnp.bfloat16)


def absorb(running, queries, key_piece, causal):
    key_rows, value_rows = (key_piece[0], key_piece[1])
    map_width = queries[0].shape[-1]
    updated = []
    for branch in range(2):
        peak_old, total_old, sum_old = running[branch]
        block_keys = key_rows[:, :, branch * map_width : (branch + 1) * map_width]
        scores = jnp.einsum(
            "fqd,fkd->fqk", queries[branch], block_keys, preferred_element_type=jnp.float32
        ) * map_width ** (-0.5)
        scores = jnp.where(causal, scores, -HUGE)
        block_peak = jnp.max(scores, axis=-1)
        weights = jnp.exp(scores - block_peak[:, :, None])
        block_total = jnp.sum(weights, axis=-1)
        block_sum = jnp.einsum(
            "fqk,fkv->fqv",
            weights.astype(jnp.bfloat16),
            value_rows,
            preferred_element_type=jnp.float32,
        )
        new_peak = jnp.maximum(peak_old, block_peak)
        before = jnp.exp(peak_old - new_peak)
        after = jnp.exp(block_peak - new_peak)
        updated.append(
            (
                new_peak,
                total_old * before + block_total * after,
                sum_old * before[:, :, None] + block_sum * after[:, :, None],
            )
        )
    return tuple(updated)


def empty_running(seq_count, row_count, head_size):
    return (
        jnp.full((seq_count, row_count), -HUGE, jnp.float32),
        jnp.zeros((seq_count, row_count), jnp.float32),
        jnp.zeros((seq_count, row_count, head_size), jnp.float32),
    )


def pack_running(running):
    return jnp.stack(
        [
            jnp.concatenate([member[2], member[0][:, :, None], member[1][:, :, None]], axis=-1)
            for member in running
        ]
    )


def unpack_running(packed):
    return tuple(
        (
            (packed[branch, :, :, -2], packed[branch, :, :, -1], packed[branch, :, :, :-2])
            for branch in range(2)
        )
    )


def local(
    tokens,
    in_gain,
    ret_query,
    ret_key,
    ret_value,
    decay_log,
    init_state,
    ret_gain,
    diff_query,
    diff_key,
    diff_value,
    diff_lambda,
    diff_gain,
    out_weight,
):
    head_size = ret_query.shape[1]
    map_size = diff_query.shape[2]
    model_width = tokens.shape[1]
    seq_count = 1
    position = lax.axis_index(SP)
    stacked = jnp.concatenate(
        [
            ret_query,
            ret_key,
            ret_value,
            diff_query[0],
            diff_query[1],
            diff_key[0],
            diff_key[1],
            diff_value,
        ],
        axis=1,
    )
    normed = norm_rows(gathered_copies(tokens, ("fs", "tp"), 0), in_gain)
    projected = jnp.dot(normed, stacked, preferred_element_type=jnp.float32).astype(jnp.bfloat16)[
        None
    ]
    rows_dev = projected.shape[1]
    bounds = [
        0,
        head_size,
        2 * head_size,
        3 * head_size,
        3 * head_size + map_size,
        3 * head_size + 2 * map_size,
        3 * head_size + 3 * map_size,
        3 * head_size + 4 * map_size,
        4 * head_size + 4 * map_size,
    ]
    pieces = [projected[:, :, bounds[slot] : bounds[slot + 1]] for slot in range(8)]
    ret_queries, ret_keys, ret_values = (pieces[0], pieces[1], pieces[2])
    first_query, second_query, first_key, second_key, diff_values = (
        pieces[3],
        pieces[4],
        pieces[5],
        pieces[6],
        pieces[7],
    )
    blocks = rows_dev // RBLOCK

    def split_blocks(array):
        return array.reshape((seq_count, blocks, RBLOCK) + array.shape[2:])

    block_queries = split_blocks(ret_queries)
    block_keys = split_blocks(ret_keys)
    block_values = split_blocks(ret_values)
    cumulative_decay = jnp.cumsum(split_blocks(decay_log), axis=-1)
    lower = jnp.arange(RBLOCK)[:, None] >= jnp.arange(RBLOCK)[None, :]
    gaps = jnp.where(
        lower, cumulative_decay[:, :, :, None] - cumulative_decay[:, :, None, :], -HUGE
    )
    scores = (
        jnp.einsum("fbik,fbjk->fbij", block_queries, block_keys, preferred_element_type=jnp.float32)
        * head_size ** (-0.5)
        * jnp.exp(gaps)
    )
    inner = jnp.einsum(
        "fbij,fbjv->fbiv",
        scores.astype(jnp.bfloat16),
        block_values,
        preferred_element_type=jnp.float32,
    )
    scaled_queries = block_queries.astype(jnp.float32) * jnp.exp(cumulative_decay)[:, :, :, None]
    ending_index = cumulative_decay[:, :, -1]
    key_weights = jnp.exp(ending_index[:, :, None] - cumulative_decay) * head_size ** (-0.5)
    block_states = jnp.einsum(
        "fbik,fbiv->fbkv",
        block_keys.astype(jnp.float32) * key_weights[:, :, :, None],
        block_values.astype(jnp.float32),
        precision=UPPER_LIMIT,
    )
    block_decay = jnp.exp(ending_index)
    local_state = jnp.zeros((seq_count, head_size, head_size), jnp.float32)
    decay_before = jnp.ones((seq_count,), jnp.float32)
    cross_parts = [
        jnp.einsum("fik,fkv->fiv", scaled_queries[:, 0], local_state, precision=UPPER_LIMIT)
    ]
    decays = [decay_before]
    local_state = block_decay[:, 0, None, None] * local_state + block_states[:, 0]
    decay_before = decay_before * block_decay[:, 0]
    start_state = init_state.astype(jnp.float32)
    first_device = position == 0

    def pack_link(decay_value, state_value):
        decay_row = jnp.broadcast_to(decay_value[:, None, None], (seq_count, 1, head_size))
        return jnp.concatenate([state_value, decay_row], axis=1)

    element = pack_link(
        jnp.where(first_device, 0.0, decay_before),
        jnp.where(
            first_device, decay_before[:, None, None] * start_state + local_state, local_state
        ),
    )

    def link(earlier, later):
        later_decay = later[:, head_size:, :]
        return jnp.concatenate(
            [
                later_decay[:, :, :1] * earlier[:, :head_size, :] + later[:, :head_size, :],
                earlier[:, head_size:, :] * later_decay,
            ],
            axis=1,
        )

    identity = pack_link(
        jnp.ones((seq_count,), jnp.float32),
        jnp.zeros((seq_count, head_size, head_size), jnp.float32),
    )
    prefix = prefix_by_axis(element, SP, link, identity)
    entering = jnp.where(first_device, start_state, prefix[:, :head_size, :])
    carried_state = (
        jnp.einsum("fbik,fkv->fbiv", scaled_queries, entering, precision=UPPER_LIMIT)
        * jnp.stack(decays, axis=1)[:, :, None, None]
    )
    ret_out = (inner + jnp.stack(cross_parts, axis=1) + carried_state).reshape(
        seq_count, rows_dev, head_size
    )
    centre = ret_out - jnp.mean(ret_out, axis=-1, keepdims=True)
    ret_mix = (
        centre * lax.rsqrt(jnp.mean(centre * centre, axis=-1, keepdims=True) + EPS) * ret_gain
    ).astype(jnp.bfloat16)
    query_places = position * rows_dev + jnp.arange(rows_dev)
    queries = (first_query, second_query)
    own_piece = jnp.stack([jnp.concatenate([first_key, second_key], axis=-1), diff_values])
    empty_sums = empty_running(seq_count, rows_dev, head_size)
    piece = lax.all_gather(own_piece, SP, axis=2, tiled=True)
    count = piece.shape[2]

    def ingest_portion(packed_in):
        allowed = jnp.arange(count)[None, :] <= query_places[:, None]
        return pack_running(absorb(unpack_running(packed_in), queries, piece, allowed))

    folded = lax.cond(
        jnp.int32(0) <= query_places[-1],
        ingest_portion,
        lambda packed_in: packed_in,
        pack_running((empty_sums, empty_sums)),
    )
    running = unpack_running(folded)
    diff_out = (
        running[0][2] / running[0][1][:, :, None]
        - diff_lambda[0] * running[1][2] / running[1][1][:, :, None]
    )
    diff_mix = (
        diff_out
        * lax.rsqrt(jnp.mean(diff_out * diff_out, axis=-1, keepdims=True) + EPS)
        * diff_gain
    ).astype(jnp.bfloat16)
    mixed_heads = jnp.concatenate([ret_mix, diff_mix], axis=-1).reshape(-1, 2 * head_size)
    full_weight = gathered_copies(out_weight, SP, 2).reshape(2 * head_size, model_width)
    own_rows = tokens.shape[0]
    picked = lax.slice_in_dim(mixed_heads, 0, own_rows * lax.axis_size(("fs", "tp")), axis=0)
    summed = sum_at_owner(
        jnp.dot(picked, full_weight, preferred_element_type=jnp.float32).astype(jnp.bfloat16),
        ("fs", "tp"),
        0,
    )
    return summed.astype(jnp.bfloat16)


def solution(mesh):
    split = Mesh(
        mesh.devices.reshape(8, 8, mesh.shape["fs"], mesh.shape["tp"]), ("sp_0", "sp_1", "fs", "tp")
    )
    placed = (
        P(SP_FS_TP, None),
        P(),
        P(None, ("fs", "tp")),
        P(None, ("fs", "tp")),
        P(None, ("fs", "tp")),
        P(("fs", "tp"), SP),
        P(("fs", "tp"), None, None),
        P(("fs", "tp")),
        P(None, None, ("fs", "tp")),
        P(None, None, ("fs", "tp")),
        P(None, ("fs", "tp")),
        P(("fs", "tp")),
        P(("fs", "tp")),
        P(None, ("fs", "tp"), SP),
    )
    return jax.shard_map(
        local, mesh=split, in_specs=placed, out_specs=P(SP_FS_TP, None), check_vma=False
    )
```

profile of v0, /device:TPU:1, one launch (start us, length us, event | category | flops | bytes accessed | tf_op | source)
XLA Modules:
  0.0 171.5 jit_solution(16919975328179489663)
XLA Ops:
  6.5 1.7 %broadcast_in_dim.22 = bf16[8,16,2048]{2,1,0:T(8,128)(2,1)} broadcast(bf16[16,2048]{1,0:T(8,128)(2,1)} %param.16), dimensions={1,2} | broadcast | bytes 589824 | tf_op jit(solution)/shard_map/broadcast_in_dim | solution.py:19
  8.3 10.9 %all-to-all-start = ((bf16[8,16,2048]{2,1,0:T(8,128)(2,1)}), bf16[8,16,2048]{2,1,0:T(8,128)(2,1)}, u32[]{:S(2)}, u32[]{:S(2)}) async-start(bf16[8,16,2048]{2,1,0:T(8,128)(2,1)} %broadcast_in_dim.22), calls=%async_computation | async-start | bytes 1048576 | tf_op jit(solution)/shard_map/all_to_all | solution.py:19
  19.2 1.1 fusion.150
  20.2 1.0 copy.35
  21.2 1.0 copy.36
  22.3 1.0 copy.37
  23.3 1.0 copy.38
  24.3 4.9 %concatenate.210 = bf16[2048,768]{1,0:T(8,128)(2,1)S(1)} concatenate(bf16[2048,128]{1,0:T(8,128)(2,1)} %param.18, bf16[2048,128]{1,0:T(8,128)(2,1)} %param.19, bf16[2048,128]{1,0:T(8,128)(2,1)} %param.20, bf16[2048,64]{1,0:T(8,128)(2,1)} %bitcast.247, bf16[2048,64]{1,0:T(8,128)(2,1)} %bitcast.248, bf16[2048,64]{1,0:T(8,128)(2,1)} %bitcast.249, bf16[2048,64]{1,0:T(8,128)(2,1)} %bitcast.250, ...), dimensions={1} | concatenate | bytes 6291456 | tf_op jit(solution)/shard_map/concatenate | solution.py:150
  29.3 1.2 multiply_reduce_fusion
  30.5 0.1 rsqrt.28
  30.6 0.0 copy-start.8
  30.6 0.0 copy-start.3
  30.6 1.2 fusion.68
  31.9 0.6 fusion.60
  32.5 0.0 copy-start.2
  32.5 0.6 pad_maximum_fusion.11
  33.2 0.0 all-gather.3.cloned.1.call-update
  33.2 2.0 %broadcast_in_dim.26 = bf16[64,2,128,32]{2,1,3,0:T(2,128)(2,1)} broadcast(bf16[2,128,32]{1,0,2:T(2,128)(2,1)S(1)} %copy.34), dimensions={1,2,3} | broadcast | bytes 1064960 | tf_op jit(solution)/shard_map/broadcast_in_dim | solution.py:19
  35.2 11.4 %all-to-all-start.1 = ((bf16[64,2,128,32]{2,1,3,0:T(2,128)(2,1)}), bf16[64,2,128,32]{2,1,3,0:T(2,128)(2,1)S(1)}, u32[]{:S(2)}, u32[]{:S(2)}) async-start(bf16[64,2,128,32]{2,1,3,0:T(2,128)(2,1)} %broadcast_in_dim.26), calls=%async_computation.1 | async-start | bytes 2097152 | tf_op jit(solution)/shard_map/all_to_all | solution.py:19
  46.6 0.7 slice.359
  48.6 0.3 reduce_window_sum.11
  48.9 0.7 slice.291
  50.3 0.6 exponential_multiply_fusion
  50.9 0.3 fusion.69
  51.3 36.7 %all-gather = bf16[8,129,128]{2,1,0:T(8,128)(2,1)S(1)} all-gather(bf16[1,129,128]{2,1,0:T(8,128)(2,1)S(1)} %concatenate.211), channel_id=2, replica_groups=mesh['sp_0'=8,'sp_1'=8,'fs'=4,'tp'=2] {'sp_1'}, dimensions={0}, use_global_device_ids=true | all-gather | bytes 297216 | tf_op jit(solution)/shard_map/all_gather | solution.py:42
  88.0 0.6 slice.379
  88.6 0.5 slice.381
  89.1 0.5 slice.383
  89.6 0.5 slice.385
  90.2 0.5 slice.387
  90.7 0.6 slice.389
  91.2 0.5 slice.391
  91.8 0.6 slice.393
  93.0 4.4 %convert_bitcast_fusion.1 = (bf16[1,1,128,128]{3,2,1,0:T(8,128)(2,1)S(1)}, f32[1,128,128]{2,1,0:T(8,128)S(1)}, f32[1,128,128]{2,1,0:T(8,128)S(1)}, f32[1,128,128...) fusion(f32[1,129,128]{2,1,0:T(8,128)S(1)} %get-tuple-element.87, ...), kind=kLoop, calls=%fused_computation.183 | loop fusion | flops 262144 | bytes 1081376 | tf_op jit(solution)/shard_map/concatenate | solution.py:246
  97.4 21.8 %all_gather.15 = bf16[8,1,129,128]{3,2,1,0:T(8,128)(2,1)S(1)} all-gather(bf16[1,1,129,128]{3,2,1,0:T(8,128)(2,1)S(1)} %pad_maximum_fusion.12), channel_id=1, replica_groups=mesh['sp_0'=8,'sp_1'=8,'fs'=4,'tp'=2] {'sp_0'}, dimensions={0}, use_global_device_ids=true | all-gather | bytes 297216 | tf_op jit(solution)/shard_map/all_gather | solution.py:42
  119.2 0.6 slice.412
  119.8 0.5 slice.414
  120.3 0.5 slice.416
  120.9 0.5 slice.418
  121.4 0.5 slice.420
  121.9 0.6 slice.422
  122.4 0.5 slice.424
  123.0 0.6 slice.426
  124.3 0.6 slice.410
  124.9 0.3 fusion.64
  125.2 0.3 convolution_add_fusion.2
  125.5 4.4 %slice_add_fusion = (f32[1,128,128]{2,1,0:T(8,128)S(1)}, f32[1,128,128]{2,1,0:T(8,128)S(1)}, f32[1,128,128]{2,1,0:T(8,128)S(1)}, f32[1,128,128]{2,1,0:T(8,128)S(...) fusion(f32[1,129,128]{2,1,0:T(8,128)S(1)} %get-tuple-element.79, ...), kind=kLoop, calls=%fused_computation.121 | loop fusion | flops 245760 | bytes 1048608 | tf_op jit(solution)/shard_map/add | solution.py:248
  130.0 1.0 fusion.151
  131.0 0.1 fusion.112
  131.1 0.0 all-gather.3.cloned.1.call-done
  131.2 0.0 copy-start.7
  131.2 8.5 %conditional.1 = (f32[2,1,128,130]{2,3,1,0:T(8,128)S(1)}) conditional(s32[]{:T(128)} %bitcast.74, () %tuple.11, (s32[128]{0:T(128)S(1)}, bf16[1,128,768]{2,1,0:T(8,128)(2,1)S(1)}, bf16[2,1,8192,128]{3,2,1,0:T(8,128)(2,1)}) %tuple.12), branch_computations={%region_4.5_spmd, %region_5.10_spmd} | conditional | flops 822251008 | bytes 55269412 | solution.py:282
  131.2 1.7 %slice_bitcast_fusion.4 = bf16[1,8192,128]{2,1,0:T(8,128)(2,1)S(1)} fusion(bf16[2,1,8192,128]{3,2,1,0:T(8,128)(2,1)} %get-tuple-element.19), kind=kLoop, calls=%fused_computation.19 | loop fusion | bytes 4194304 | tf_op jit(solution)/shard_map/cond/branch_1_fun/squeeze | solution.py:71
  132.9 0.9 fusion.148
  133.9 0.8 fusion.2
  134.7 0.5 copy-done
  135.1 1.1 fusion.26
  136.2 1.5 fusion.147
  137.7 0.8 fusion.4
  138.5 1.1 fusion.41
  139.8 0.1 multiply_convert_fusion
  139.9 0.5 convolution_convert_fusion
  140.4 23.6 %all_to_all.15 = bf16[8,16,2048]{2,1,0:T(8,128)(2,1)S(1)} all-to-all(bf16[8,16,2048]{2,1,0:T(8,128)(2,1)S(1)} %bitcast.251), channel_id=1, replica_groups=mesh['sp_0'=8,'sp_1'=8,'fs'=4,'tp'=2] {'fs','tp'}, dimensions={0} | all-to-all | bytes 1048576 | tf_op jit(solution)/shard_map/all_to_all | solution.py:60
  164.0 0.7 reduce_sum.74
  (41 shorter events, 0.5 us)
Async XLA Ops:
  6.5 15.7 %copy-start.1 = (bf16[2,2048,64]{1,2,0:T(8,128)(2,1)S(1)}, bf16[2,2048,64]{1,2,0:T(8,128)(2,1)}, u32[]{:S(2)}) copy-start(bf16[2,2048,64]{1,2,0:T(8,128)(2,1)} %param.25) | copy-start | bytes 1572868
  8.3 21.0 %all-to-all-start = ((bf16[8,16,2048]{2,1,0:T(8,128)(2,1)}), bf16[8,16,2048]{2,1,0:T(8,128)(2,1)}, u32[]{:S(2)}, u32[]{:S(2)}) async-start(bf16[8,16,2048]{2,1,0:T(8,128)(2,1)} %broadcast_in_dim.22), calls=%async_computation | async-start | bytes 1048576 | tf_op jit(solution)/shard_map/all_to_all | solution.py:19
  19.2 112.0 %all-gather.3.cloned.1.call-start = ((), (), s32[]{:S(2)}) async-start(), calls=%async_computation.3 | async-start | bytes 4259840 | tf_op jit(solution)/shard_map/all_gather | solution.py:275
  23.3 7.3 %copy-start.5 = (f32[2048]{0:T(1024)S(1)}, f32[2048]{0:T(1024)}, u32[]{:S(2)}) copy-start(f32[2048]{0:T(1024)} %param.17) | copy-start | bytes 24580
  29.3 3.9 %copy-start.4 = (bf16[2,128,32]{1,2,0:T(8,128)(2,1)S(1)}, bf16[2,128,32]{1,2,0:T(8,128)(2,1)}, u32[]{:S(2)}) copy-start(bf16[2,128,32]{1,2,0:T(8,128)(2,1)} %param.29) | copy-start | bytes 49156
  30.6 18.0 %copy-start.8 = (f32[1,128]{1,0:T(1,128)S(1)}, f32[1,128]{1,0:T(1,128)}, u32[]{:S(2)}) copy-start(f32[1,128]{1,0:T(1,128)} %param.21) | copy-start | bytes 1540
  30.6 20.3 %copy-start.3 = (bf16[1,128,128]{2,1,0:T(8,128)(2,1)S(1)}, bf16[1,128,128]{2,1,0:T(8,128)(2,1)}, u32[]{:S(2)}) copy-start(bf16[1,128,128]{2,1,0:T(8,128)(2,1)} %param.22) | copy-start | bytes 98308
  32.5 91.8 %copy-start.2 = (f32[1,129,128]{2,1,0:T(8,128)S(1)}, f32[1,129,128]{2,1,0:T(8,128)}, u32[]{:S(2)}) copy-start(f32[1,129,128]{2,1,0:T(8,128)} %constant.89.clone.1) | copy-start | bytes 198148
  35.2 95.8 %copy-start.6 = (f32[128]{0:T(128)S(1)}, f32[128]{0:T(128)}, u32[]{:S(2)}) copy-start(f32[128]{0:T(128)} %param.23) | copy-start | bytes 1540
  35.2 104.7 %all-to-all-start.1 = ((bf16[64,2,128,32]{2,1,3,0:T(2,128)(2,1)}), bf16[64,2,128,32]{2,1,3,0:T(2,128)(2,1)S(1)}, u32[]{:S(2)}, u32[]{:S(2)}) async-start(bf16[64,2,128,32]{2,1,3,0:T(2,128)(2,1)} %broadcast_in_dim.26), calls=%async_computation.1 | async-start | bytes 2097152 | tf_op jit(solution)/shard_map/all_to_all | solution.py:19
  131.2 8.6 %copy-start.7 = (f32[128]{0:T(128)S(1)}, f32[128]{0:T(128)}, u32[]{:S(2)}) copy-start(f32[128]{0:T(128)} %param.28) | copy-start | bytes 1540
  132.9 2.2 %copy-start = (bf16[2,1,8192,128]{3,2,1,0:T(8,128)(2,1)S(1)}, bf16[2,1,8192,128]{3,2,1,0:T(8,128)(2,1)}, u32[]{:S(2)}) copy-start(bf16[2,1,8192,128]{3,2,1,0:T(8,128)(2,1)} %get-tuple-element.19) | copy-start | bytes 12582916 | tf_op jit(solution)/shard_map/cond
Sparse Core Ops, SparseCore 0:
  33.3 96.4 all-gather.2
where the time goes:
time: 172 us
  blocking collectives  82 us (48%)
  local copies, waits for them, and re-layouts  26.7 us (16%)
  starting transfers between devices  22.2 us (13%)
  between operations  17.1 us (10%)
  other arithmetic  15.7 us (9%)
  matrix products  7.7 us (4%)
    all_gather x2, blocking collectives, prefix_by_axis(): pieces = lax.all_gather(total.astype(jnp.bfloat16), axis)  58.4 us
    all_to_all x1, blocking collectives, sum_at_owner(): pieces = lax.all_to_all(cut_along(x, dim, size), axis, 0, 0, tiled=True)  23.6 us
    all_to_all x2, starting transfers between devices, from_everyone(): lax.all_to_all(jnp.broadcast_to(x[None], (size, *x.shape)), axis, 0, 0, t...  22.2 us
    slice x17, local copies, waits for them, and re-layouts, link(): later_decay[:, :, :1] * earlier[:, :head_size, :] + later[:, :head_size, :]  9.23 us
    concatenate x1, local copies, waits for them, and re-layouts, local(): jnp.concatenate([ret_query, ret_key, ret_value, diff_query[0], diff_query...  4.94 us
    concatenate x3, other arithmetic, link(): jnp.concatenate([later_decay[:, :, :1] * earlier[:, :head_size, :] + late...  4.45 us
    add x1, other arithmetic, link(): later_decay[:, :, :1] * earlier[:, :head_size, :] + later[:, :head_size, :]  4.43 us
    unnamed x21, local copies, waits for them, and re-layouts  4.11 us
  transfers between devices with their start and end apart: 3, of which 0 were waited for; matrix products, arithmetic and copies ran while one was open for 25% of the time, Pallas kernels for 0%

commit v1 on v0

v1 whole, which is shorter than its diff:
```python
import functools

import jax
import jax.numpy as jnp
from jax import lax
from jax.experimental import pallas as pl
from jax.experimental.pallas import tpu as pltpu
from jax.sharding import Mesh
from jax.sharding import PartitionSpec as P

SP = ("sp_0", "sp_1")
SP_FS_TP = ("sp_0", "sp_1", "fs", "tp")
MESH = pl.DeviceIdType.MESH
EPS = 1e-06
HUGE = 1e30
FLOOR = -1e29
BLK = 128
BF = jnp.bfloat16
F32 = jnp.float32
HIGH = lax.Precision.HIGHEST


def dot(a, b, **kw):
    return jnp.dot(a, b, preferred_element_type=F32, **kw)


def dot_nt(a, b):
    return lax.dot_general(a, b, (((1,), (1,)), ((), ())), preferred_element_type=F32)


def iota(shape, dim):
    return lax.broadcasted_iota(jnp.int32, shape, dim)


def kernel(
    dims,
    tok_h, gain_h, wrq_h, wrk_h, wrv_h, dec_h, init_h, rgain_h, wq_h, wk_h, wv_h, lam_s, dgain_h, ow_h,
    out_ref,
    tok, gain, dec, init, rgain, dgain, wqk, w, x,
    kall, vtall, qbuf, so, st, ro, rst,
    sa, sda, ra, rda, sb, sdb, rb, rdb, sc, rc,
    wsm, wbig, fs, fr,
    in_sem, tok_ss, tok_rs, ow_ss, ow_rs, kf_ss, kf_rs, kb_ss, kb_rs, q_ss, q_rs,
    a_ss, a_rs, b_ss, b_rs, c_ss, c_rs, r_ss, r_rs, wf_ss, wf_rs, wb_ss, wb_rs, f_ss, f_rs,
):
    nz, ny, nx, nc = dims
    nh = nx * nc
    rows = BLK // nh
    sl = BLK // ny
    nf, nb = nz // 2, nz - 1 - nz // 2
    z, y = lax.axis_index("sp_0"), lax.axis_index("sp_1")
    fx, c = lax.axis_index("fs"), lax.axis_index("tp")
    h = fx * nc + c

    def head_peer(d):
        p = lax.rem(h + d, nh)
        return p, (z, y, p // nc, lax.rem(p, nc))

    def y_peer(d):
        p = lax.rem(y + d, ny)
        return p, (z, p, fx, c)

    def z_peer(d):
        p = lax.rem(z + d, nz)
        return p, (p, y, fx, c)

    def rcopy(src, dst, ss, rs, dev):
        return pltpu.make_async_remote_copy(
            src_ref=src, dst_ref=dst, send_sem=ss, recv_sem=rs, device_id=dev, device_id_type=MESH
        )

    barrier = pltpu.get_barrier_semaphore()
    for d in range(1, nh):
        pl.semaphore_signal(barrier, inc=1, device_id=head_peer(d)[1], device_id_type=MESH)
    for d in range(1, ny):
        pl.semaphore_signal(barrier, inc=1, device_id=y_peer(d)[1], device_id_type=MESH)
    for d in range(1, nz):
        pl.semaphore_signal(barrier, inc=1, device_id=z_peer(d)[1], device_id_type=MESH)

    own_w = wsm.at[:, pl.ds(pl.multiple_of(y * 32, 32), 32), :]
    inputs = [
        (tok_h, tok), (gain_h, gain), (ow_h, own_w), (wk_h, wqk.at[0]), (wq_h, wqk.at[1]),
        (wv_h, w.at[:, pl.ds(128, 128)]), (wrq_h, w.at[:, pl.ds(384, 128)]),
        (wrk_h, w.at[:, pl.ds(512, 128)]), (wrv_h, w.at[:, pl.ds(640, 128)]),
        (dec_h, dec), (init_h, init), (rgain_h, rgain), (dgain_h, dgain),
    ]
    loads = [pltpu.make_async_copy(s, t, in_sem.at[i]) for i, (s, t) in enumerate(inputs)]
    for copy in loads:
        copy.start()

    loads[0].wait()
    loads[1].wait()
    t = tok[...].astype(F32)
    scale = lax.rsqrt(jnp.mean(t * t, axis=-1, keepdims=True) + EPS)
    own_x = x.at[pl.ds(pl.multiple_of(h * rows, rows), rows), :]
    own_x[...] = (t * scale * gain[...]).astype(BF)
    loads[2].wait()

    pl.semaphore_wait(barrier, nh + ny + nz - 3)

    sends = []

    def go(copy):
        copy.start()
        sends.append(copy)

    for d in range(1, nh):
        go(rcopy(own_x, own_x, tok_ss.at[d], tok_rs.at[d], head_peer(d)[1]))
    for d in range(1, ny):
        go(rcopy(own_w, own_w, ow_ss.at[d], ow_rs.at[d], y_peer(d)[1]))

    loads[3].wait()
    w[:, 0:128] = wqk[0].astype(F32).T.astype(BF)
    loads[4].wait()
    w[:, 256:384] = wqk[1].astype(F32).T.astype(BF)
    for copy in loads[5:]:
        copy.wait()

    row, col = iota((BLK, BLK), 0), iota((BLK, BLK), 1)
    lower = row >= col
    decb = jnp.broadcast_to(dec[...], (BLK, BLK))
    cum_col = jnp.sum(jnp.where(lower, decb, 0.0), axis=1, keepdims=True)
    dec_col = jnp.sum(jnp.where(row == col, decb, 0.0), axis=1, keepdims=True)
    cum_row = jnp.sum(jnp.where(row <= col, jnp.broadcast_to(dec_col, (BLK, BLK)), 0.0), axis=0, keepdims=True)
    cum_end = jnp.sum(dec[...], axis=1, keepdims=True)
    fade = jnp.exp(jnp.where(lower, cum_col - cum_row, -HUGE)) * (BLK ** (-0.5))
    key_weight = jnp.exp(cum_end - cum_col) * (BLK ** (-0.5))
    reach = jnp.exp(cum_col)
    sda[...] = jnp.broadcast_to(jnp.exp(cum_end), sda.shape)

    for d in range(1, nh):
        p, dev = head_peer(nh - d)
        part = x.at[pl.ds(pl.multiple_of(p * rows, rows), rows), :]
        rcopy(part, part, tok_ss.at[d], tok_rs.at[d], dev).wait_recv()

    xs = x[...]
    kv = dot(xs, w[:, 0:256])
    kall[0:BLK, :] = kv[:, 0:128].astype(BF)
    vtall[:, 0:BLK] = kv[:, 128:256].T.astype(BF)

    def k_at(s):
        return kall.at[pl.ds(s * BLK, BLK), :]

    def v_at(s):
        return vtall.at[:, pl.ds(s * BLK, BLK)]

    right, left = z_peer(1)[1], z_peer(nz - 1)[1]

    def kv_hop(s, forward, part):
        if forward:
            src, dst, ss, rs, dev = s - 1, s, kf_ss, kf_rs, right
        else:
            src, dst, ss, rs, dev = (0 if s == 1 else nf + s - 1), nf + s, kb_ss, kb_rs, left
        at = (k_at, v_at)[part]
        return rcopy(at(src), at(dst), ss.at[s - 1, part], rs.at[s - 1, part], dev)

    def kv_start(s):
        for part in range(2):
            if s <= nf:
                go(kv_hop(s, True, part))
            if s <= nb:
                go(kv_hop(s, False, part))

    def kv_advance(s):
        for part in range(2):
            if s <= nf:
                kv_hop(s, True, part).wait_recv()
                if s + 1 <= nf:
                    go(kv_hop(s + 1, True, part))
            if s <= nb:
                kv_hop(s, False, part).wait_recv()
                if s + 1 <= nb:
                    go(kv_hop(s + 1, False, part))

    kv_start(1)

    rest = dot(xs, w[:, 256:768])
    qbuf[0] = (rest[:, 0:128].astype(BF).astype(F32) * (64 ** (-0.5))).T.astype(BF)
    for d in range(1, ny):
        go(rcopy(qbuf.at[0], qbuf.at[d], q_ss.at[d], q_rs.at[d], y_peer(d)[1]))

    rq, rk, rv = (rest[:, 128 * i : 128 * (i + 1)].astype(BF) for i in (1, 2, 3))
    keyed = (rk.astype(F32) * key_weight).T
    state = dot(keyed, rv.astype(F32), precision=HIGH)
    sa[...] = state.reshape(ny, sl, BLK)
    ra[pl.ds(y, 1)] = sa[pl.ds(y, 1)]
    rda[pl.ds(y, 1)] = sda[...].reshape(1, 1, BLK)
    for d in range(1, ny):
        p, dev = y_peer(d)
        go(rcopy(sa.at[p], ra.at[y], a_ss.at[d, 0], a_rs.at[d, 0], dev))
        go(rcopy(sda, rda.at[y], a_ss.at[d, 1], a_rs.at[d, 1], dev))

    kv_advance(1)
    scores = dot_nt(rq, rk) * fade
    inner = dot(scores.astype(BF), rv)
    reaching = rq.astype(F32) * reach

    kv_advance(2)

    for d in range(1, ny):
        p, dev = y_peer(ny - d)
        part = wsm.at[:, pl.ds(pl.multiple_of(p * 32, 32), 32), :]
        rcopy(part, part, ow_ss.at[d], ow_rs.at[d], dev).wait_recv()
    for i in range(2):
        wbig[pl.ds(z, 1), i * 128 : (i + 1) * 128, :] = wsm[i].astype(F32).T.astype(BF)[None]

    for s in range(3, nf):
        kv_advance(s)

    for d in range(1, ny):
        p, dev = y_peer(ny - d)
        rcopy(sa.at[p], ra.at[p], a_ss.at[d, 0], a_rs.at[d, 0], dev).wait_recv()
        rcopy(sda, rda.at[p], a_ss.at[d, 1], a_rs.at[d, 1], dev).wait_recv()
    total = ra[0]
    decay = rda[0]
    for i in range(1, ny):
        total = rda[i] * total + ra[i]
        decay = decay * rda[i]
    sb[...] = total
    sdb[...] = decay
    rb[pl.ds(z, 1)] = jnp.zeros((1, sl, BLK), F32)
    rdb[pl.ds(z, 1)] = jnp.zeros((1, 1, BLK), F32)
    for d in range(1, nz):
        dev = z_peer(d)[1]
        go(rcopy(sb, rb.at[z], b_ss.at[d, 0], b_rs.at[d, 0], dev))
        go(rcopy(sdb, rdb.at[z], b_ss.at[d, 1], b_rs.at[d, 1], dev))

    if nf > 2:
        kv_advance(nf)

    def ow_hop(s, half, forward):
        if forward:
            slot, ss, rs, dev = lax.rem(z + nz - s + 1, nz), wf_ss, wf_rs, right
        else:
            slot, ss, rs, dev = lax.rem(z + s - 1, nz), wb_ss, wb_rs, left
        ref = wbig.at[slot, pl.ds(half * 128, 128), :]
        return rcopy(ref, ref, ss.at[s - 1, half], rs.at[s - 1, half], dev)

    def ow_wait(s, half, forward):
        if forward:
            slot, ss, rs, dev = lax.rem(z + nz - s, nz), wf_ss, wf_rs, right
        else:
            slot, ss, rs, dev = lax.rem(z + s, nz), wb_ss, wb_rs, left
        ref = wbig.at[slot, pl.ds(half * 128, 128), :]
        rcopy(ref, ref, ss.at[s - 1, half], rs.at[s - 1, half], dev).wait_recv()

    def ow_start(s):
        for half in range(2):
            if s <= nf:
                go(ow_hop(s, half, True))
            if s <= nb:
                go(ow_hop(s, half, False))

    def ow_advance(s):
        for half in range(2):
            if s <= nf:
                ow_wait(s, half, True)
                if s + 1 <= nf:
                    go(ow_hop(s + 1, half, True))
            if s <= nb:
                ow_wait(s, half, False)
                if s + 1 <= nb:
                    go(ow_hop(s + 1, half, False))

    ow_start(1)

    for d in range(1, ny):
        rcopy(qbuf.at[0], qbuf.at[d], q_ss.at[d], q_rs.at[d], y_peer(ny - d)[1]).wait_recv()

    def finish_states():
        for d in range(1, nz):
            p, dev = z_peer(nz - d)
            rcopy(sb, rb.at[p], b_ss.at[d, 0], b_rs.at[d, 0], dev).wait_recv()
            rcopy(sdb, rdb.at[p], b_ss.at[d, 1], b_rs.at[d, 1], dev).wait_recv()
        entry = init[0, pl.ds(pl.multiple_of(y * sl, sl), sl), :].astype(F32)
        for i in range(nz):
            entry = jnp.where(i < z, rdb[i] * entry + rb[i], entry)
        for i in range(ny):
            sc[i] = entry
            entry = rda[i] * entry + ra[i]
        rc[pl.ds(y, 1)] = sc[pl.ds(y, 1)]
        for d in range(1, ny):
            p, dev = y_peer(d)
            rcopy(sc.at[p], rc.at[y], c_ss.at[d], c_rs.at[d], dev).start()

    krow, lane = iota((BLK, 2 * BLK), 0), iota((BLK, 2 * BLK), 1)
    qlane = jnp.where(lane >= BLK, lane - BLK, lane)
    valid = [None] + [jnp.where(s <= z, 0.0, -HUGE) for s in range(1, nf + 1)]
    valid += [jnp.where(z + s >= nz, 0.0, -HUGE) for s in range(1, nb + 1)]

    def attend(i, _):
        k = (i + 1) // 2
        d = lax.rem(ny // 2 + (2 * lax.rem(i, 2) - 1) * k + 2 * ny, ny)
        yq = lax.rem(y - d + ny, ny)
        q = qbuf[d]
        zero = jnp.zeros_like(q)
        top_half = row < 64
        qt = jnp.concatenate([jnp.where(top_half, q, zero), jnp.where(top_half, zero, q)], axis=1)
        s = dot(kall[...], qt)
        pieces = [jnp.where(krow + y * BLK <= qlane + yq * BLK, s[0:BLK], -HUGE)]
        for n in range(1, nz):
            pieces.append(s[n * BLK : (n + 1) * BLK] + valid[n])
        s = jnp.concatenate(pieces, axis=0)
        peak = jnp.maximum(jnp.max(s, axis=0, keepdims=True), FLOOR)
        p = jnp.exp(s - peak)
        st[pl.ds(d, 1), 0:1, :] = peak[None]
        st[pl.ds(d, 1), 1:2, :] = jnp.sum(p, axis=0, keepdims=True)[None]
        so[pl.ds(d, 1)] = dot(vtall[...], p.astype(BF)).astype(BF)[None]

        @pl.when(i < ny - 1)
        def _():
            dev = (z, yq, fx, c)
            rcopy(so.at[d], ro.at[d], r_ss.at[d, 0], r_rs.at[d, 0], dev).start()
            rcopy(st.at[d], rst.at[d], r_ss.at[d, 1], r_rs.at[d, 1], dev).start()

        @pl.when(i == ny // 2)
        def _():
            finish_states()

        return 0

    lax.fori_loop(0, ny, attend, 0)

    for s in range(1, nf + 1):
        ow_advance(s)

    for d in range(1, ny):
        p, dev = y_peer(ny - d)
        rcopy(sc.at[p], rc.at[p], c_ss.at[d], c_rs.at[d], dev).wait_recv()
    ret = inner + dot(reaching, rc[...].reshape(BLK, BLK), precision=HIGH)
    centre = ret - jnp.mean(ret, axis=-1, keepdims=True)
    ret_mix = (
        centre * lax.rsqrt(jnp.mean(centre * centre, axis=-1, keepdims=True) + EPS) * rgain[...]
    ).astype(BF)

    for d in range(1, ny):
        dev = y_peer(d)[1]
        rcopy(so.at[d], ro.at[d], r_ss.at[d, 0], r_rs.at[d, 0], dev).wait_recv()
        rcopy(st.at[d], rst.at[d], r_ss.at[d, 1], r_rs.at[d, 1], dev).wait_recv()
    stats = [st[0]] + [rst[d] for d in range(1, ny)]
    top = stats[0][0:1]
    for one in stats[1:]:
        top = jnp.maximum(top, one[0:1])
    total = jnp.zeros_like(top)
    merged = jnp.zeros((BLK, 2 * BLK), F32)
    for d in range(ny):
        share = jnp.exp(stats[d][0:1] - top)
        total = total + share * stats[d][1:2]
        merged = merged + (so[0] if d == 0 else ro[d]).astype(F32) * share
    merged = merged / total
    diff = merged[:, 0:128] - lam_s[0] * merged[:, 128:256]
    diff = diff * lax.rsqrt(jnp.mean(diff * diff, axis=0, keepdims=True) + EPS)
    diff_mix = (diff.T * dgain[...]).astype(BF)

    mix = jnp.concatenate([ret_mix, diff_mix], axis=1)
    wide = wbig.shape[2]
    for i in range(nz):
        fs[:, i * wide : (i + 1) * wide] = dot(mix, wbig[i]).astype(BF)
    for d in range(1, nh):
        p, dev = head_peer(d)
        part = fs.at[pl.ds(pl.multiple_of(p * rows, rows), rows), :]
        go(rcopy(part, fr.at[d], f_ss.at[d], f_rs.at[d], dev))
    acc = fs[pl.ds(pl.multiple_of(h * rows, rows), rows), :].astype(F32)
    for d in range(1, nh):
        dev = head_peer(d)[1]
        rcopy(own_x, fr.at[d], f_ss.at[d], f_rs.at[d], dev).wait_recv()
        acc = acc + fr[d].astype(F32)
    out_ref[...] = acc.astype(BF)

    for copy in sends:
        copy.wait_send()
    for d in range(1, ny):
        p, dev = y_peer(d)
        rcopy(sc.at[p], rc.at[y], c_ss.at[d], c_rs.at[d], dev).wait_send()
        rcopy(so.at[d], ro.at[d], r_ss.at[d, 0], r_rs.at[d, 0], dev).wait_send()
        rcopy(st.at[d], rst.at[d], r_ss.at[d, 1], r_rs.at[d, 1], dev).wait_send()


def local(
    dims, tokens, in_gain, ret_query, ret_key, ret_value, decay_log, init_state, ret_gain,
    diff_query, diff_key, diff_value, diff_lambda, diff_gain, out_weight,
):
    nz, ny, nx, nc = dims
    nh = nx * nc
    rows, width = tokens.shape
    sl = BLK // ny
    nf, nb = nz // 2, nz - 1 - nz // 2
    dma = pltpu.SemaphoreType.DMA
    vm = pltpu.VMEM
    scratch = [
        vm((rows, width), BF), vm((1, width), F32), vm((1, BLK), F32), vm((1, BLK, BLK), BF),
        vm((1, BLK), F32), vm((1, BLK), F32), vm((2, BLK, width), BF), vm((width, 768), BF), vm((BLK, width), BF),
        vm((nz * BLK, BLK), BF), vm((BLK, nz * BLK), BF), vm((ny, BLK, BLK), BF),
        vm((ny, BLK, 2 * BLK), BF), vm((ny, 2, 2 * BLK), F32), vm((ny, BLK, 2 * BLK), BF), vm((ny, 2, 2 * BLK), F32),
        vm((ny, sl, BLK), F32), vm((1, BLK), F32), vm((ny, sl, BLK), F32), vm((ny, 1, BLK), F32),
        vm((sl, BLK), F32), vm((1, BLK), F32), vm((nz, sl, BLK), F32), vm((nz, 1, BLK), F32),
        vm((ny, sl, BLK), F32), vm((ny, sl, BLK), F32),
        vm((2, 32 * ny, BLK), BF), vm((nz, 2 * BLK, 32 * ny), BF), vm((BLK, width), BF), vm((nh, rows, width), BF),
        dma((13,)), dma((nh,)), dma((nh,)), dma((ny,)), dma((ny,)),
        dma((nf, 2)), dma((nf, 2)), dma((max(nb, 1), 2)), dma((max(nb, 1), 2)), dma((ny,)), dma((ny,)),
        dma((ny, 2)), dma((ny, 2)), dma((nz, 2)), dma((nz, 2)), dma((ny,)), dma((ny,)),
        dma((ny, 2)), dma((ny, 2)), dma((nf, 2)), dma((nf, 2)), dma((max(nb, 1), 2)), dma((max(nb, 1), 2)),
        dma((nh,)), dma((nh,)),
    ]
    anyspec = pl.BlockSpec(memory_space=pl.ANY)
    smem = pl.BlockSpec(memory_space=pltpu.SMEM)
    return pl.pallas_call(
        functools.partial(kernel, dims),
        out_shape=jax.ShapeDtypeStruct((rows, width), BF),
        in_specs=[anyspec] * 11 + [smem] + [anyspec] * 2,
        out_specs=pl.BlockSpec(memory_space=pltpu.VMEM),
        scratch_shapes=scratch,
        compiler_params=pltpu.CompilerParams(
            collective_id=0, has_side_effects=True, vmem_limit_bytes=60 * 1024 * 1024
        ),
    )(
        tokens,
        in_gain.reshape(1, width),
        ret_query,
        ret_key,
        ret_value,
        decay_log,
        init_state,
        ret_gain.reshape(1, BLK),
        jnp.swapaxes(diff_query, 1, 2).reshape(BLK, width),
        jnp.swapaxes(diff_key, 1, 2).reshape(BLK, width),
        diff_value,
        diff_lambda,
        diff_gain.reshape(1, BLK),
        jnp.swapaxes(out_weight, 1, 2),
    )


def build(split):
    dims = tuple(split.shape[a] for a in SP_FS_TP)
    placed = (
        P(SP_FS_TP, None),
        P(),
        P(None, ("fs", "tp")),
        P(None, ("fs", "tp")),
        P(None, ("fs", "tp")),
        P(("fs", "tp"), SP),
        P(("fs", "tp"), None, None),
        P(("fs", "tp")),
        P(None, None, ("fs", "tp")),
        P(None, None, ("fs", "tp")),
        P(None, ("fs", "tp")),
        P(("fs", "tp")),
        P(("fs", "tp")),
        P(None, ("fs", "tp"), SP),
    )
    return jax.shard_map(
        functools.partial(local, dims), mesh=split, in_specs=placed, out_specs=P(SP_FS_TP, None), check_vma=False
    )


def solution(mesh):
    return build(Mesh(mesh.devices.reshape(8, 8, mesh.shape["fs"], mesh.shape["tp"]), SP_FS_TP))
```

time: 172 us -> 67.6 us (0.39)
  blocking collectives: 82 us -> 0 us
  Pallas kernels: 0 us -> 65.3 us
  local copies, waits for them, and re-layouts: 26.7 us -> 1.47 us
  starting transfers between devices: 22.2 us -> 0 us
  between operations: 17.1 us -> 0.66 us
  other arithmetic: 15.7 us -> 0 us
  matrix products: 7.7 us -> 0 us
    pallas_call x0 -> x1, Pallas kernels: none -> 65.3 us  [local(): pl.pallas_call(functools.partial(kernel, dims), out_shape=jax.ShapeDtypeS...]
    all_gather x2 -> x0, blocking collectives: 58.4 us -> none  [prefix_by_axis(): pieces = lax.all_gather(total.astype(jnp.bfloat16), axis)]
    all_to_all x1 -> x0, blocking collectives: 23.6 us -> none  [sum_at_owner(): pieces = lax.all_to_all(cut_along(x, dim, size), axis, 0, 0, tiled=True)]
    all_to_all x2 -> x0, starting transfers between devices: 22.2 us -> none  [from_everyone(): lax.all_to_all(jnp.broadcast_to(x[None], (size, *x.shape)), axis, 0, 0, t...]
    slice x21 -> x0, local copies, waits for them, and re-layouts: 11.6 us -> none  [the longest x17 9.23 us: link(): later_decay[:, :, :1] * earlier[:, :head_size, :] + later[:, :head_size, :]]
    dot_general x10 -> x0, matrix products: 7.7 us -> none  [the longest x2 2.42 us: absorb(): jnp.einsum('fqd,fkd->fqk', queries[branch], block_keys, preferred_element...]
    concatenate x2 -> x0, local copies, waits for them, and re-layouts: 4.95 us -> none  [the longest x1 4.94 us: local(): jnp.concatenate([ret_query, ret_key, ret_value, diff_query[0], diff_query...]
    concatenate x3 -> x0, other arithmetic: 4.45 us -> none  [link(): jnp.concatenate([later_decay[:, :, :1] * earlier[:, :head_size, :] + late...]
  transfers between devices with their start and end apart: 3 -> 0, of which waited for: 0 -> 0; matrix products, arithmetic and copies ran while one was open for 25% -> 0% of each run, Pallas kernels for 0% -> 0%
where the time goes in v1:
time: 67.6 us; the launch traced here: 67.5 us
  Pallas kernels  65.3 us (97%)
  local copies, waits for them, and re-layouts  1.47 us (2%)
    pallas_call x1, Pallas kernels, local(): pl.pallas_call(functools.partial(kernel, dims), out_shape=jax.ShapeDtypeS...  65.3 us
    unnamed x1, local copies, waits for them, and re-layouts  1.47 us

profile of v1, /device:TPU:1, one launch (start us, length us, event | category | flops | bytes accessed | tf_op | source)
XLA Modules:
  0.0 67.5 jit_solution(1064057676030942782)
XLA Ops:
  0.7 65.3 %shard_map.136 = bf16[16,2048]{1,0:T(8,128)(2,1)} custom-call(bf16[16,2048]{1,0:T(8,128)(2,1)} %tok_h.1, f32[1,2048]{1,0:T(1,128)} %bitcast.13, bf16[2048,128]{1,0:T(8,128)(2,1)} %wrq_h.1, bf16[2048,128]{1,0:T(8,128)(2,1)} %wrk_h.1, bf16[2048,128]{1,0:T(8,128)(2,1)} %wrv_h.1, f32[1,128]{1,0:T(1,128)} %dec_h.1, bf16[1,128,128]{2,1,0:T(8,128)(2,1)} %init_h.1, ...), custom_call_target="tpu_custom_call" | custom-call | tf_op jit(solution)/shard_map/pallas_call | solution.py:407
  66.0 1.5 %copy.17 = bf16[16,2048]{1,0:T(8,128)(2,1)} copy(bf16[16,2048]{1,0:T(8,128)(2,1)} %shard_map.136) | data formatting | bytes 131072

commit v2 on v1

--- a/solution.py
+++ b/solution.py
@@ -39,15 +39,16 @@
     tok, gain, dec, init, rgain, dgain, wqk, w, x,
     kall, vtall, qbuf, so, st, ro, rst,
     sa, sda, ra, rda, sb, sdb, rb, rdb, sc, rc,
-    wsm, wbig, fs, fr,
-    in_sem, tok_ss, tok_rs, ow_ss, ow_rs, kf_ss, kf_rs, kb_ss, kb_rs, q_ss, q_rs,
-    a_ss, a_rs, b_ss, b_rs, c_ss, c_rs, r_ss, r_rs, wf_ss, wf_rs, wb_ss, wb_rs, f_ss, f_rs,
+    early_sum, early_stat, wt, pwt, wpair, mixb, pmix, fs, fr,
+    in_sem, tok_ss, tok_rs, pt_ss, pt_rs, ow_ss, ow_rs, kf_ss, kf_rs, kb_ss, kb_rs, q_ss, q_rs,
+    a_ss, a_rs, b_ss, b_rs, c_ss, c_rs, r_ss, r_rs, wf_ss, wf_rs, wb_ss, wb_rs, pw_ss, pw_rs, mix_ss, mix_rs, f_ss, f_rs,
 ):
     nz, ny, nx, nc = dims
     nh = nx * nc
     rows = BLK // nh
     sl = BLK // ny
     nf, nb = nz // 2, nz - 1 - nz // 2
+    early = 5 if nz > 5 else 3
     z, y = lax.axis_index("sp_0"), lax.axis_index("sp_1")
     fx, c = lax.axis_index("fs"), lax.axis_index("tp")
     h = fx * nc + c
@@ -55,6 +56,26 @@
     def head_peer(d):
         p = lax.rem(h + d, nh)
         return p, (z, y, p // nc, lax.rem(p, nc))
+
+    a, b = (1 - c) * z + c * y, (1 - c) * y + c * z
+
+    def a_place(p):
+        return z + (1 - c) * (p - a), y + c * (p - a)
+
+    def b_place(p):
+        return z + c * (p - b), y + (1 - c) * (p - b)
+
+    def a_peer(d):
+        return (*a_place(lax.rem(a + d, nz)), fx, c)
+
+    def b_peer(d):
+        return (*b_place(lax.rem(b + d, nz)), fx, c)
+
+    def x_peer(d):
+        p = lax.rem(fx + d, nx)
+        return p, (z, y, p, c)
+
+    partner = (z, y, fx, 1 - c)
 
     def y_peer(d):
         p = lax.rem(y + d, ny)
@@ -77,9 +98,8 @@
     for d in range(1, nz):
         pl.semaphore_signal(barrier, inc=1, device_id=z_peer(d)[1], device_id_type=MESH)
 
-    own_w = wsm.at[:, pl.ds(pl.multiple_of(y * 32, 32), 32), :]
     inputs = [
-        (tok_h, tok), (gain_h, gain), (ow_h, own_w), (wk_h, wqk.at[0]), (wq_h, wqk.at[1]),
+        (tok_h, tok), (gain_h, gain), (ow_h, wt.at[:, z, y]), (wk_h, wqk.at[0]), (wq_h, wqk.at[1]),
         (wv_h, w.at[:, pl.ds(128, 128)]), (wrq_h, w.at[:, pl.ds(384, 128)]),
         (wrk_h, w.at[:, pl.ds(512, 128)]), (wrv_h, w.at[:, pl.ds(640, 128)]),
         (dec_h, dec), (init_h, init), (rgain_h, rgain), (dgain_h, dgain),
@@ -104,10 +124,18 @@
         copy.start()
         sends.append(copy)
 
-    for d in range(1, nh):
-        go(rcopy(own_x, own_x, tok_ss.at[d], tok_rs.at[d], head_peer(d)[1]))
-    for d in range(1, ny):
-        go(rcopy(own_w, own_w, ow_ss.at[d], ow_rs.at[d], y_peer(d)[1]))
+    def x_rows(p, core):
+        return x.at[pl.ds(pl.multiple_of((p * nc + core) * rows, rows), rows), :]
+
+    for d in range(1, nx):
+        go(rcopy(own_x, own_x, tok_ss.at[d], tok_rs.at[d], x_peer(d)[1]))
+    if nc > 1:
+        go(rcopy(own_x, own_x, pt_ss.at[0], pt_rs.at[0], partner))
+    for d in range(1, ny):
+        part = wt.at[0, z, y]
+        go(rcopy(part, part, ow_ss.at[d, 0], ow_rs.at[d, 0], y_peer(d)[1]))
+        part = wt.at[1, z, y]
+        go(rcopy(part, part, ow_ss.at[d, 1], ow_rs.at[d, 1], z_peer(d)[1]))
 
     loads[3].wait()
     w[:, 0:128] = wqk[0].astype(F32).T.astype(BF)
@@ -128,10 +156,16 @@
     reach = jnp.exp(cum_col)
     sda[...] = jnp.broadcast_to(jnp.exp(cum_end), sda.shape)
 
-    for d in range(1, nh):
-        p, dev = head_peer(nh - d)
-        part = x.at[pl.ds(pl.multiple_of(p * rows, rows), rows), :]
+    for d in sorted(range(1, nx), key=lambda v: min(v, nx - v)):
+        p, dev = x_peer(nx - d)
+        part = x_rows(p, c)
         rcopy(part, part, tok_ss.at[d], tok_rs.at[d], dev).wait_recv()
+        if nc > 1:
+            go(rcopy(part, part, pt_ss.at[d], pt_rs.at[d], partner))
+    if nc > 1:
+        for d in range(nx):
+            part = x_rows(lax.rem(fx + nx - d, nx), 1 - c)
+            rcopy(part, part, pt_ss.at[d], pt_rs.at[d], partner).wait_recv()
 
     xs = x[...]
     kv = dot(xs, w[:, 0:256])
@@ -144,13 +178,13 @@
     def v_at(s):
         return vtall.at[:, pl.ds(s * BLK, BLK)]
 
-    right, left = z_peer(1)[1], z_peer(nz - 1)[1]
+    right, left = a_peer(1), a_peer(nz - 1)
 
     def kv_hop(s, forward, part):
         if forward:
-            src, dst, ss, rs, dev = s - 1, s, kf_ss, kf_rs, right
+            src, dst, ss, rs, dev = max(2 * s - 3, 0), 2 * s - 1, kf_ss, kf_rs, right
         else:
-            src, dst, ss, rs, dev = (0 if s == 1 else nf + s - 1), nf + s, kb_ss, kb_rs, left
+            src, dst, ss, rs, dev = 2 * s - 2, 2 * s, kb_ss, kb_rs, left
         at = (k_at, v_at)[part]
         return rcopy(at(src), at(dst), ss.at[s - 1, part], rs.at[s - 1, part], dev)
 
@@ -177,7 +211,7 @@
     rest = dot(xs, w[:, 256:768])
     qbuf[0] = (rest[:, 0:128].astype(BF).astype(F32) * (64 ** (-0.5))).T.astype(BF)
     for d in range(1, ny):
-        go(rcopy(qbuf.at[0], qbuf.at[d], q_ss.at[d], q_rs.at[d], y_peer(d)[1]))
+        go(rcopy(qbuf.at[0], qbuf.at[d], q_ss.at[d], q_rs.at[d], b_peer(d)))
 
     rq, rk, rv = (rest[:, 128 * i : 128 * (i + 1)].astype(BF) for i in (1, 2, 3))
     keyed = (rk.astype(F32) * key_weight).T
@@ -190,22 +224,55 @@
         go(rcopy(sa.at[p], ra.at[y], a_ss.at[d, 0], a_rs.at[d, 0], dev))
         go(rcopy(sda, rda.at[y], a_ss.at[d, 1], a_rs.at[d, 1], dev))
 
+    for d in range(1, ny):
+        part = wt.at[0, z, y_peer(ny - d)[0]]
+        rcopy(part, part, ow_ss.at[d, 0], ow_rs.at[d, 0], partner).wait_recv()
+        part = wt.at[1, z_peer(nz - d)[0], y]
+        rcopy(part, part, ow_ss.at[d, 1], ow_rs.at[d, 1], partner).wait_recv()
+
+    def ow_hop(s, half, forward, arriving=False):
+        place, peer = ((z, z_peer), (y, y_peer))[half]
+        back = s if arriving else s - 1
+        slot = lax.rem(place + (nz - back if forward else back), nz)
+        ref = wt.at[0, slot] if half == 0 else wt.at[1, :, slot]
+        ss, rs = (wf_ss, wf_rs) if forward else (wb_ss, wb_rs)
+        return rcopy(ref, ref, ss.at[s - 1, half], rs.at[s - 1, half], peer(1 if forward else nz - 1)[1])
+
+    def ow_start(s):
+        for half in range(2):
+            if s <= nf:
+                go(ow_hop(s, half, True))
+            if s <= nb:
+                go(ow_hop(s, half, False))
+
+    def ow_wait(s):
+        for half in range(2):
+            if s <= nf:
+                ow_hop(s, half, True, True).wait_recv()
+            if s <= nb:
+                ow_hop(s, half, False, True).wait_recv()
+
+    def ow_share(n, half):
+        place = (z, y)[half]
+        slot = lax.rem(place + (nz - (n + 1) // 2 if n % 2 else n // 2), nz)
+        src, dst = (wt.at[0, slot], pwt.at[0, slot]) if half == 0 else (wt.at[1, :, slot], pwt.at[1, :, slot])
+        return rcopy(src, dst, pw_ss.at[n, half], pw_rs.at[n, half], partner)
+
+    def ow_pass(s):
+        if nc > 1:
+            for n in (2 * s - 1, 2 * s) if s else (0,):
+                if n < nz:
+                    for half in range(2):
+                        ow_share(n, half).start()
+
+    ow_start(1)
+    ow_pass(0)
     kv_advance(1)
     scores = dot_nt(rq, rk) * fade
     inner = dot(scores.astype(BF), rv)
     reaching = rq.astype(F32) * reach
 
     kv_advance(2)
-
-    for d in range(1, ny):
-        p, dev = y_peer(ny - d)
-        part = wsm.at[:, pl.ds(pl.multiple_of(p * 32, 32), 32), :]
-        rcopy(part, part, ow_ss.at[d], ow_rs.at[d], dev).wait_recv()
-    for i in range(2):
-        wbig[pl.ds(z, 1), i * 128 : (i + 1) * 128, :] = wsm[i].astype(F32).T.astype(BF)[None]
-
-    for s in range(3, nf):
-        kv_advance(s)
 
     for d in range(1, ny):
         p, dev = y_peer(ny - d)
@@ -225,104 +292,130 @@
         go(rcopy(sb, rb.at[z], b_ss.at[d, 0], b_rs.at[d, 0], dev))
         go(rcopy(sdb, rdb.at[z], b_ss.at[d, 1], b_rs.at[d, 1], dev))
 
-    if nf > 2:
-        kv_advance(nf)
-
-    def ow_hop(s, half, forward):
-        if forward:
-            slot, ss, rs, dev = lax.rem(z + nz - s + 1, nz), wf_ss, wf_rs, right
-        else:
-            slot, ss, rs, dev = lax.rem(z + s - 1, nz), wb_ss, wb_rs, left
-        ref = wbig.at[slot, pl.ds(half * 128, 128), :]
-        return rcopy(ref, ref, ss.at[s - 1, half], rs.at[s - 1, half], dev)
-
-    def ow_wait(s, half, forward):
-        if forward:
-            slot, ss, rs, dev = lax.rem(z + nz - s, nz), wf_ss, wf_rs, right
-        else:
-            slot, ss, rs, dev = lax.rem(z + s, nz), wb_ss, wb_rs, left
-        ref = wbig.at[slot, pl.ds(half * 128, 128), :]
-        rcopy(ref, ref, ss.at[s - 1, half], rs.at[s - 1, half], dev).wait_recv()
-
-    def ow_start(s):
-        for half in range(2):
-            if s <= nf:
-                go(ow_hop(s, half, True))
-            if s <= nb:
-                go(ow_hop(s, half, False))
-
-    def ow_advance(s):
-        for half in range(2):
-            if s <= nf:
-                ow_wait(s, half, True)
-                if s + 1 <= nf:
-                    go(ow_hop(s + 1, half, True))
-            if s <= nb:
-                ow_wait(s, half, False)
-                if s + 1 <= nb:
-                    go(ow_hop(s + 1, half, False))
-
-    ow_start(1)
-
-    for d in range(1, ny):
-        rcopy(qbuf.at[0], qbuf.at[d], q_ss.at[d], q_rs.at[d], y_peer(ny - d)[1]).wait_recv()
-
-    def finish_states():
-        for d in range(1, nz):
-            p, dev = z_peer(nz - d)
-            rcopy(sb, rb.at[p], b_ss.at[d, 0], b_rs.at[d, 0], dev).wait_recv()
-            rcopy(sdb, rdb.at[p], b_ss.at[d, 1], b_rs.at[d, 1], dev).wait_recv()
-        entry = init[0, pl.ds(pl.multiple_of(y * sl, sl), sl), :].astype(F32)
-        for i in range(nz):
-            entry = jnp.where(i < z, rdb[i] * entry + rb[i], entry)
-        for i in range(ny):
-            sc[i] = entry
-            entry = rda[i] * entry + ra[i]
-        rc[pl.ds(y, 1)] = sc[pl.ds(y, 1)]
-        for d in range(1, ny):
-            p, dev = y_peer(d)
-            rcopy(sc.at[p], rc.at[y], c_ss.at[d], c_rs.at[d], dev).start()
+    ow_wait(1)
+    if nf > 1:
+        ow_start(2)
+    ow_pass(1)
+    for d in range(1, ny):
+        rcopy(qbuf.at[0], qbuf.at[d], q_ss.at[d], q_rs.at[d], b_peer(ny - d)).wait_recv()
 
     krow, lane = iota((BLK, 2 * BLK), 0), iota((BLK, 2 * BLK), 1)
     qlane = jnp.where(lane >= BLK, lane - BLK, lane)
-    valid = [None] + [jnp.where(s <= z, 0.0, -HUGE) for s in range(1, nf + 1)]
-    valid += [jnp.where(z + s >= nz, 0.0, -HUGE) for s in range(1, nb + 1)]
-
-    def attend(i, _):
-        k = (i + 1) // 2
-        d = lax.rem(ny // 2 + (2 * lax.rem(i, 2) - 1) * k + 2 * ny, ny)
-        yq = lax.rem(y - d + ny, ny)
-        q = qbuf[d]
-        zero = jnp.zeros_like(q)
-        top_half = row < 64
-        qt = jnp.concatenate([jnp.where(top_half, q, zero), jnp.where(top_half, zero, q)], axis=1)
-        s = dot(kall[...], qt)
-        pieces = [jnp.where(krow + y * BLK <= qlane + yq * BLK, s[0:BLK], -HUGE)]
-        for n in range(1, nz):
-            pieces.append(s[n * BLK : (n + 1) * BLK] + valid[n])
-        s = jnp.concatenate(pieces, axis=0)
-        peak = jnp.maximum(jnp.max(s, axis=0, keepdims=True), FLOOR)
-        p = jnp.exp(s - peak)
-        st[pl.ds(d, 1), 0:1, :] = peak[None]
-        st[pl.ds(d, 1), 1:2, :] = jnp.sum(p, axis=0, keepdims=True)[None]
-        so[pl.ds(d, 1)] = dot(vtall[...], p.astype(BF)).astype(BF)[None]
-
-        @pl.when(i < ny - 1)
-        def _():
-            dev = (z, yq, fx, c)
+    steps = [0] + [(nz - (s + 1) // 2 if s % 2 else s // 2) for s in range(1, nz)]
+    places = [a_place(lax.rem(a + step, nz)) for step in steps]
+    key_blocks = [kz * ny + ky for kz, ky in places]
+    top_half = row < 64
+
+    def pair(i):
+        return nz // 2 - i, lax.rem(nz // 2 + 1 + i, nz)
+
+    def attend(i, lo, hi):
+        places, wide = [], []
+        for d in pair(i):
+            places.append(b_place(lax.rem(b - d + nz, nz)))
+            q = qbuf[d]
+            zero = jnp.zeros_like(q)
+            wide += [jnp.where(top_half, q, zero), jnp.where(top_half, zero, q)]
+        blocks = [qz * ny + qy for qz, qy in places]
+        s_all = dot(kall[lo * BLK : hi * BLK, :], jnp.concatenate(wide, axis=1))
+        probs, peaks, totals = [], [], []
+        for n in range(2):
+            pieces = []
+            for m in range(lo, hi):
+                s = s_all[(m - lo) * BLK : (m - lo + 1) * BLK, n * 256 : (n + 1) * 256]
+                if m == 0:
+                    s = jnp.where(krow + key_blocks[0] * BLK <= qlane + blocks[n] * BLK, s, -HUGE)
+                else:
+                    s = s + jnp.where(key_blocks[m] < blocks[n], 0.0, -HUGE)
+                pieces.append(s)
+            s = jnp.concatenate(pieces, axis=0)
+            peak = jnp.max(s, axis=0, keepdims=True)
+            if lo == 0:
+                peak = jnp.maximum(peak, FLOOR)
+            else:
+                peak = jnp.maximum(peak, early_stat[i, 0:1, n * 256 : (n + 1) * 256])
+            p = jnp.exp(s - peak)
+            peaks.append(peak)
+            totals.append(jnp.sum(p, axis=0, keepdims=True))
+            probs.append(p.astype(BF))
+        sums = dot(vtall[:, lo * BLK : hi * BLK], jnp.concatenate(probs, axis=1))
+        return sums, jnp.concatenate(peaks, axis=1), jnp.concatenate(totals, axis=1), places
+
+    def attend_early(i, _):
+        sums, peak, total, _ = attend(i, 0, early)
+        early_sum[pl.ds(i, 1)] = sums[None]
+        early_stat[pl.ds(i, 1)] = jnp.concatenate([peak, total], axis=0)[None]
+        return 0
+
+    def attend_late(i, _):
+        first, second = pair(i)
+        sums, peak, total, places = attend(i, early, nz)
+        share = jnp.exp(early_stat[i, 0:1, :] - peak)
+        total = total + share * early_stat[i, 1:2, :]
+        sums = (sums + share * early_sum[i]).astype(BF)
+        stat = jnp.concatenate([peak, total], axis=0)
+        so[pl.ds(first, 1)] = sums[None, :, 0:256]
+        so[pl.ds(second, 1)] = sums[None, :, 256:512]
+        st[pl.ds(first, 1)] = stat[None, :, 0:256]
+        st[pl.ds(second, 1)] = stat[None, :, 256:512]
+
+        def send(d, place):
+            dev = (*place, fx, c)
             rcopy(so.at[d], ro.at[d], r_ss.at[d, 0], r_rs.at[d, 0], dev).start()
             rcopy(st.at[d], rst.at[d], r_ss.at[d, 1], r_rs.at[d, 1], dev).start()
 
-        @pl.when(i == ny // 2)
+        send(first, places[0])
+
+        @pl.when(i < nz // 2 - 1)
         def _():
-            finish_states()
+            send(second, places[1])
 
         return 0
 
-    lax.fori_loop(0, ny, attend, 0)
-
-    for s in range(1, nf + 1):
-        ow_advance(s)
+    lax.fori_loop(0, nz // 4, attend_early, 0)
+    if nf > 2:
+        kv_advance(3)
+    lax.fori_loop(nz // 4, nz // 2, attend_early, 0)
+    for s in range(4, nf + 1):
+        kv_advance(s)
+
+    for d in range(1, nz):
+        p, dev = z_peer(nz - d)
+        rcopy(sb, rb.at[p], b_ss.at[d, 0], b_rs.at[d, 0], dev).wait_recv()
+        rcopy(sdb, rdb.at[p], b_ss.at[d, 1], b_rs.at[d, 1], dev).wait_recv()
+    entry = init[0, pl.ds(pl.multiple_of(y * sl, sl), sl), :].astype(F32)
+    for i in range(nz):
+        entry = jnp.where(i < z, rdb[i] * entry + rb[i], entry)
+    for i in range(ny):
+        sc[i] = entry
+        entry = rda[i] * entry + ra[i]
+    rc[pl.ds(y, 1)] = sc[pl.ds(y, 1)]
+    for d in range(1, ny):
+        p, dev = y_peer(d)
+        rcopy(sc.at[p], rc.at[y], c_ss.at[d], c_rs.at[d], dev).start()
+
+    if nf > 2:
+        ow_wait(2)
+        ow_start(3)
+        ow_pass(2)
+    lax.fori_loop(0, nz // 2, attend_late, 0)
+    for s in range(3, nf):
+        ow_wait(s)
+        ow_start(s + 1)
+        ow_pass(s)
+
+
+    width = out_ref.shape[1]
+    ow_wait(nf)
+    ow_pass(nf)
+    for half in range(2):
+        wpair[half * BLK : (half + 1) * BLK, :] = wt[half].reshape(width, BLK).astype(F32).T.astype(BF)
+    if nc > 1:
+        for n in range(nz):
+            for half in range(2):
+                ow_share(n, half).wait_recv()
+        for half in range(2):
+            wpair[(2 + half) * BLK : (3 + half) * BLK, :] = pwt[half].reshape(width, BLK).astype(F32).T.astype(BF)
 
     for d in range(1, ny):
         p, dev = y_peer(ny - d)
@@ -334,9 +427,8 @@
     ).astype(BF)
 
     for d in range(1, ny):
-        dev = y_peer(d)[1]
-        rcopy(so.at[d], ro.at[d], r_ss.at[d, 0], r_rs.at[d, 0], dev).wait_recv()
-        rcopy(st.at[d], rst.at[d], r_ss.at[d, 1], r_rs.at[d, 1], dev).wait_recv()
+        rcopy(so.at[d], ro.at[d], r_ss.at[d, 0], r_rs.at[d, 0], b_peer(d)).wait_recv()
+        rcopy(st.at[d], rst.at[d], r_ss.at[d, 1], r_rs.at[d, 1], b_peer(d)).wait_recv()
     stats = [st[0]] + [rst[d] for d in range(1, ny)]
     top = stats[0][0:1]
     for one in stats[1:]:
@@ -353,27 +445,34 @@
     diff_mix = (diff.T * dgain[...]).astype(BF)
 
     mix = jnp.concatenate([ret_mix, diff_mix], axis=1)
-    wide = wbig.shape[2]
-    for i in range(nz):
-        fs[:, i * wide : (i + 1) * wide] = dot(mix, wbig[i]).astype(BF)
-    for d in range(1, nh):
-        p, dev = head_peer(d)
-        part = fs.at[pl.ds(pl.multiple_of(p * rows, rows), rows), :]
-        go(rcopy(part, fr.at[d], f_ss.at[d], f_rs.at[d], dev))
-    acc = fs[pl.ds(pl.multiple_of(h * rows, rows), rows), :].astype(F32)
-    for d in range(1, nh):
-        dev = head_peer(d)[1]
-        rcopy(own_x, fr.at[d], f_ss.at[d], f_rs.at[d], dev).wait_recv()
+    mixb[...] = mix.reshape(nx, nc, rows, 256)
+    if nc > 1:
+        swap = rcopy(mixb.at[:, 1 - c], pmix, mix_ss, mix_rs, partner)
+        go(swap)
+        swap.wait_recv()
+        mine = mixb[:, pl.ds(c, 1)].reshape(nx * rows, 256)
+        mix = jnp.concatenate([mine, pmix[...].reshape(nx * rows, 256)], axis=1)
+    fs[...] = dot(mix, wpair[...]).astype(BF).reshape(nx, rows, width)
+    for d in range(1, nx):
+        p, dev = x_peer(d)
+        go(rcopy(fs.at[p], fr.at[d], f_ss.at[d], f_rs.at[d], dev))
+    acc = fs[pl.ds(fx, 1)].reshape(rows, width).astype(F32)
+    for d in range(1, nx):
+        rcopy(fs.at[0], fr.at[d], f_ss.at[d], f_rs.at[d], x_peer(d)[1]).wait_recv()
         acc = acc + fr[d].astype(F32)
     out_ref[...] = acc.astype(BF)
 
     for copy in sends:
         copy.wait_send()
+    if nc > 1:
+        for n in range(nz):
+            for half in range(2):
+                ow_share(n, half).wait_send()
     for d in range(1, ny):
         p, dev = y_peer(d)
         rcopy(sc.at[p], rc.at[y], c_ss.at[d], c_rs.at[d], dev).wait_send()
-        rcopy(so.at[d], ro.at[d], r_ss.at[d, 0], r_rs.at[d, 0], dev).wait_send()
-        rcopy(st.at[d], rst.at[d], r_ss.at[d, 1], r_rs.at[d, 1], dev).wait_send()
+        rcopy(so.at[d], ro.at[d], r_ss.at[d, 0], r_rs.at[d, 0], b_peer(d)).wait_send()
+        rcopy(st.at[d], rst.at[d], r_ss.at[d, 1], r_rs.at[d, 1], b_peer(d)).wait_send()
 
 
 def local(
@@ -395,12 +494,14 @@
         vm((ny, sl, BLK), F32), vm((1, BLK), F32), vm((ny, sl, BLK), F32), vm((ny, 1, BLK), F32),
         vm((sl, BLK), F32), vm((1, BLK), F32), vm((nz, sl, BLK), F32), vm((nz, 1, BLK), F32),
         vm((ny, sl, BLK), F32), vm((ny, sl, BLK), F32),
-        vm((2, 32 * ny, BLK), BF), vm((nz, 2 * BLK, 32 * ny), BF), vm((BLK, width), BF), vm((nh, rows, width), BF),
-        dma((13,)), dma((nh,)), dma((nh,)), dma((ny,)), dma((ny,)),
+        vm((nz // 2, BLK, 4 * BLK), F32), vm((nz // 2, 2, 4 * BLK), F32),
+        vm((2, nz, ny, 32, BLK), BF), vm((2, nz, ny, 32, BLK), BF), vm((2 * nc * BLK, width), BF),
+        vm((nx, nc, rows, 2 * BLK), BF), vm((nx, rows, 2 * BLK), BF), vm((nx, rows, width), BF), vm((nx, rows, width), BF),
+        dma((13,)), dma((nx,)), dma((nx,)), dma((nx,)), dma((nx,)), dma((ny, 2)), dma((ny, 2)),
         dma((nf, 2)), dma((nf, 2)), dma((max(nb, 1), 2)), dma((max(nb, 1), 2)), dma((ny,)), dma((ny,)),
         dma((ny, 2)), dma((ny, 2)), dma((nz, 2)), dma((nz, 2)), dma((ny,)), dma((ny,)),
         dma((ny, 2)), dma((ny, 2)), dma((nf, 2)), dma((nf, 2)), dma((max(nb, 1), 2)), dma((max(nb, 1), 2)),
-        dma((nh,)), dma((nh,)),
+        dma((nz, 2)), dma((nz, 2)), dma, dma, dma((nx,)), dma((nx,)),
     ]
     anyspec = pl.BlockSpec(memory_space=pl.ANY)
     smem = pl.BlockSpec(memory_space=pltpu.SMEM)

time: 67.6 us -> 62.4 us (0.923)
  Pallas kernels: 65.3 us -> 60.1 us
    pallas_call x1, Pallas kernels: 65.3 us -> 60.1 us  [local(): pl.pallas_call(functools.partial(kernel, dims), out_shape=jax.ShapeDtypeS...]
where the time goes in v2:
time: 62.4 us; the launch traced here: 62.2 us
  Pallas kernels  60.1 us (96%)
  local copies, waits for them, and re-layouts  1.47 us (2%)
  between operations  0.66 us (1%)
    pallas_call x1, Pallas kernels, local(): pl.pallas_call(functools.partial(kernel, dims), out_shape=jax.ShapeDtypeS...  60.1 us
    unnamed x1, local copies, waits for them, and re-layouts  1.47 us

profile of v2, /device:TPU:1, one launch (start us, length us, event | category | flops | bytes accessed | tf_op | source)
XLA Modules:
  0.0 62.2 jit_solution(7780753028099242582)
XLA Ops:
  0.7 60.1 %shard_map.136 = bf16[16,2048]{1,0:T(8,128)(2,1)} custom-call(bf16[16,2048]{1,0:T(8,128)(2,1)} %tok_h.1, f32[1,2048]{1,0:T(1,128)} %bitcast.13, bf16[2048,128]{1,0:T(8,128)(2,1)} %wrq_h.1, bf16[2048,128]{1,0:T(8,128)(2,1)} %wrk_h.1, bf16[2048,128]{1,0:T(8,128)(2,1)} %wrv_h.1, f32[1,128]{1,0:T(1,128)} %dec_h.1, bf16[1,128,128]{2,1,0:T(8,128)(2,1)} %init_h.1, ...), custom_call_target="tpu_custom_call" | custom-call | tf_op jit(solution)/shard_map/pallas_call | solution.py:508
  60.8 1.5 %copy.17 = bf16[16,2048]{1,0:T(8,128)(2,1)} copy(bf16[16,2048]{1,0:T(8,128)(2,1)} %shard_map.136) | data formatting | bytes 131072

commit v3 on v2

--- a/solution.py
+++ b/solution.py
@@ -162,6 +162,50 @@
         rcopy(part, part, tok_ss.at[d], tok_rs.at[d], dev).wait_recv()
         if nc > 1:
             go(rcopy(part, part, pt_ss.at[d], pt_rs.at[d], partner))
+    for d in range(1, ny):
+        part = wt.at[0, z, y_peer(ny - d)[0]]
+        rcopy(part, part, ow_ss.at[d, 0], ow_rs.at[d, 0], partner).wait_recv()
+        part = wt.at[1, z_peer(nz - d)[0], y]
+        rcopy(part, part, ow_ss.at[d, 1], ow_rs.at[d, 1], partner).wait_recv()
+
+    def ow_hop(s, half, forward, arriving=False):
+        place, peer = ((z, z_peer), (y, y_peer))[half]
+        back = s if arriving else s - 1
+        slot = lax.rem(place + (nz - back if forward else back), nz)
+        ref = wt.at[0, slot] if half == 0 else wt.at[1, :, slot]
+        ss, rs = (wf_ss, wf_rs) if forward else (wb_ss, wb_rs)
+        return rcopy(ref, ref, ss.at[s - 1, half], rs.at[s - 1, half], peer(1 if forward else nz - 1)[1])
+
+    def ow_start(s):
+        for half in range(2):
+            if s <= nf:
+                go(ow_hop(s, half, True))
+            if s <= nb:
+                go(ow_hop(s, half, False))
+
+    def ow_wait(s):
+        for half in range(2):
+            if s <= nf:
+                ow_hop(s, half, True, True).wait_recv()
+            if s <= nb:
+                ow_hop(s, half, False, True).wait_recv()
+
+    def ow_share(n, half):
+        place = (z, y)[half]
+        slot = lax.rem(place + (nz - (n + 1) // 2 if n % 2 else n // 2), nz)
+        src, dst = (wt.at[0, slot], pwt.at[0, slot]) if half == 0 else (wt.at[1, :, slot], pwt.at[1, :, slot])
+        return rcopy(src, dst, pw_ss.at[n, half], pw_rs.at[n, half], partner)
+
+    def ow_pass(s):
+        if nc > 1:
+            for n in (2 * s - 1, 2 * s) if s else (0,):
+                if n < nz:
+                    for half in range(2):
+                        ow_share(n, half).start()
+
+    ow_start(1)
+    ow_pass(0)
+
     if nc > 1:
         for d in range(nx):
             part = x_rows(lax.rem(fx + nx - d, nx), 1 - c)
@@ -181,6 +225,9 @@
     right, left = a_peer(1), a_peer(nz - 1)
 
     def kv_hop(s, forward, part):
+        if part == 2:
+            src, dst = (s - 1, s) if forward else ((nz - s + 1) % nz, nz - s)
+            return rcopy(qbuf.at[src], qbuf.at[dst], q_ss.at[dst], q_rs.at[dst], b_peer(1 if forward else nz - 1))
         if forward:
             src, dst, ss, rs, dev = max(2 * s - 3, 0), 2 * s - 1, kf_ss, kf_rs, right
         else:
@@ -188,15 +235,15 @@
         at = (k_at, v_at)[part]
         return rcopy(at(src), at(dst), ss.at[s - 1, part], rs.at[s - 1, part], dev)
 
-    def kv_start(s):
-        for part in range(2):
+    def kv_start(s, parts):
+        for part in parts:
             if s <= nf:
                 go(kv_hop(s, True, part))
             if s <= nb:
                 go(kv_hop(s, False, part))
 
     def kv_advance(s):
-        for part in range(2):
+        for part in range(3):
             if s <= nf:
                 kv_hop(s, True, part).wait_recv()
                 if s + 1 <= nf:
@@ -206,12 +253,11 @@
                 if s + 1 <= nb:
                     go(kv_hop(s + 1, False, part))
 
-    kv_start(1)
+    kv_start(1, (0, 1))
 
     rest = dot(xs, w[:, 256:768])
     qbuf[0] = (rest[:, 0:128].astype(BF).astype(F32) * (64 ** (-0.5))).T.astype(BF)
-    for d in range(1, ny):
-        go(rcopy(qbuf.at[0], qbuf.at[d], q_ss.at[d], q_rs.at[d], b_peer(d)))
+    kv_start(1, (2,))
 
     rq, rk, rv = (rest[:, 128 * i : 128 * (i + 1)].astype(BF) for i in (1, 2, 3))
     keyed = (rk.astype(F32) * key_weight).T
@@ -224,54 +270,14 @@
         go(rcopy(sa.at[p], ra.at[y], a_ss.at[d, 0], a_rs.at[d, 0], dev))
         go(rcopy(sda, rda.at[y], a_ss.at[d, 1], a_rs.at[d, 1], dev))
 
-    for d in range(1, ny):
-        part = wt.at[0, z, y_peer(ny - d)[0]]
-        rcopy(part, part, ow_ss.at[d, 0], ow_rs.at[d, 0], partner).wait_recv()
-        part = wt.at[1, z_peer(nz - d)[0], y]
-        rcopy(part, part, ow_ss.at[d, 1], ow_rs.at[d, 1], partner).wait_recv()
-
-    def ow_hop(s, half, forward, arriving=False):
-        place, peer = ((z, z_peer), (y, y_peer))[half]
-        back = s if arriving else s - 1
-        slot = lax.rem(place + (nz - back if forward else back), nz)
-        ref = wt.at[0, slot] if half == 0 else wt.at[1, :, slot]
-        ss, rs = (wf_ss, wf_rs) if forward else (wb_ss, wb_rs)
-        return rcopy(ref, ref, ss.at[s - 1, half], rs.at[s - 1, half], peer(1 if forward else nz - 1)[1])
-
-    def ow_start(s):
-        for half in range(2):
-            if s <= nf:
-                go(ow_hop(s, half, True))
-            if s <= nb:
-                go(ow_hop(s, half, False))
-
-    def ow_wait(s):
-        for half in range(2):
-            if s <= nf:
-                ow_hop(s, half, True, True).wait_recv()
-            if s <= nb:
-                ow_hop(s, half, False, True).wait_recv()
-
-    def ow_share(n, half):
-        place = (z, y)[half]
-        slot = lax.rem(place + (nz - (n + 1) // 2 if n % 2 else n // 2), nz)
-        src, dst = (wt.at[0, slot], pwt.at[0, slot]) if half == 0 else (wt.at[1, :, slot], pwt.at[1, :, slot])
-        return rcopy(src, dst, pw_ss.at[n, half], pw_rs.at[n, half], partner)
-
-    def ow_pass(s):
-        if nc > 1:
-            for n in (2 * s - 1, 2 * s) if s else (0,):
-                if n < nz:
-                    for half in range(2):
-                        ow_share(n, half).start()
-
-    ow_start(1)
-    ow_pass(0)
     kv_advance(1)
     scores = dot_nt(rq, rk) * fade
     inner = dot(scores.astype(BF), rv)
     reaching = rq.astype(F32) * reach
 
+    ow_wait(1)
+    ow_start(2)
+    ow_pass(1)
     kv_advance(2)
 
     for d in range(1, ny):
@@ -291,13 +297,6 @@
         dev = z_peer(d)[1]
         go(rcopy(sb, rb.at[z], b_ss.at[d, 0], b_rs.at[d, 0], dev))
         go(rcopy(sdb, rdb.at[z], b_ss.at[d, 1], b_rs.at[d, 1], dev))
-
-    ow_wait(1)
-    if nf > 1:
-        ow_start(2)
-    ow_pass(1)
-    for d in range(1, ny):
-        rcopy(qbuf.at[0], qbuf.at[d], q_ss.at[d], q_rs.at[d], b_peer(ny - d)).wait_recv()
 
     krow, lane = iota((BLK, 2 * BLK), 0), iota((BLK, 2 * BLK), 1)
     qlane = jnp.where(lane >= BLK, lane - BLK, lane)
@@ -341,7 +340,8 @@
         sums = dot(vtall[:, lo * BLK : hi * BLK], jnp.concatenate(probs, axis=1))
         return sums, jnp.concatenate(peaks, axis=1), jnp.concatenate(totals, axis=1), places
 
-    def attend_early(i, _):
+    def attend_early(near, _):
+        i = nz // 2 - 1 - near
         sums, peak, total, _ = attend(i, 0, early)
         early_sum[pl.ds(i, 1)] = sums[None]
         early_stat[pl.ds(i, 1)] = jnp.concatenate([peak, total], axis=0)[None]
@@ -372,12 +372,14 @@
 
         return 0
 
-    lax.fori_loop(0, nz // 4, attend_early, 0)
-    if nf > 2:
-        kv_advance(3)
-    lax.fori_loop(nz // 4, nz // 2, attend_early, 0)
-    for s in range(4, nf + 1):
+    pairs = nz // 2
+    lax.fori_loop(0, min(2, pairs), attend_early, 0)
+    for s in range(3, nf + 1):
+        ow_wait(s - 1)
+        ow_start(s)
+        ow_pass(s - 1)
         kv_advance(s)
+        lax.fori_loop(s - 1, s, attend_early, 0)
 
     for d in range(1, nz):
         p, dev = z_peer(nz - d)
@@ -394,16 +396,7 @@
         p, dev = y_peer(d)
         rcopy(sc.at[p], rc.at[y], c_ss.at[d], c_rs.at[d], dev).start()
 
-    if nf > 2:
-        ow_wait(2)
-        ow_start(3)
-        ow_pass(2)
-    lax.fori_loop(0, nz // 2, attend_late, 0)
-    for s in range(3, nf):
-        ow_wait(s)
-        ow_start(s + 1)
-        ow_pass(s)
-
+    lax.fori_loop(0, pairs, attend_late, 0)
 
     width = out_ref.shape[1]
     ow_wait(nf)

time: 62.4 us -> 59.5 us (0.954)
  Pallas kernels: 60.1 us -> 57.2 us
    pallas_call x1, Pallas kernels: 60.1 us -> 57.2 us  [local(): pl.pallas_call(functools.partial(kernel, dims), out_shape=jax.ShapeDtypeS...]
where the time goes in v3:
time: 59.5 us; the launch traced here: 59.3 us
  Pallas kernels  57.2 us (96%)
  local copies, waits for them, and re-layouts  1.47 us (2%)
  between operations  0.66 us (1%)
    pallas_call x1, Pallas kernels, local(): pl.pallas_call(functools.partial(kernel, dims), out_shape=jax.ShapeDtypeS...  57.2 us
    unnamed x1, local copies, waits for them, and re-layouts  1.47 us

profile of v3, /device:TPU:1, one launch (start us, length us, event | category | flops | bytes accessed | tf_op | source)
XLA Modules:
  0.0 59.3 jit_solution(7206483901603366108)
XLA Ops:
  0.7 57.2 %shard_map.136 = bf16[16,2048]{1,0:T(8,128)(2,1)} custom-call(bf16[16,2048]{1,0:T(8,128)(2,1)} %tok_h.1, f32[1,2048]{1,0:T(1,128)} %bitcast.13, bf16[2048,128]{1,0:T(8,128)(2,1)} %wrq_h.1, bf16[2048,128]{1,0:T(8,128)(2,1)} %wrk_h.1, bf16[2048,128]{1,0:T(8,128)(2,1)} %wrv_h.1, f32[1,128]{1,0:T(1,128)} %dec_h.1, bf16[1,128,128]{2,1,0:T(8,128)(2,1)} %init_h.1, ...), custom_call_target="tpu_custom_call" | custom-call | tf_op jit(solution)/shard_map/pallas_call | solution.py:501
  57.8 1.5 %copy.17 = bf16[16,2048]{1,0:T(8,128)(2,1)} copy(bf16[16,2048]{1,0:T(8,128)(2,1)} %shard_map.136) | data formatting | bytes 131072

commit v4 on v3

--- a/solution.py
+++ b/solution.py
@@ -15,6 +15,7 @@
 HUGE = 1e30
 FLOOR = -1e29
 BLK = 128
+RELAY = (None, 0, 1, 2, 3)
 BF = jnp.bfloat16
 F32 = jnp.float32
 HIGH = lax.Precision.HIGHEST
@@ -127,7 +128,8 @@
     def x_rows(p, core):
         return x.at[pl.ds(pl.multiple_of((p * nc + core) * rows, rows), rows), :]
 
-    for d in range(1, nx):
+    far_first = sorted(range(1, nx), key=lambda v: -min(v, nx - v))
+    for d in far_first:
         go(rcopy(own_x, own_x, tok_ss.at[d], tok_rs.at[d], x_peer(d)[1]))
     if nc > 1:
         go(rcopy(own_x, own_x, pt_ss.at[0], pt_rs.at[0], partner))
@@ -222,47 +224,44 @@
     def v_at(s):
         return vtall.at[:, pl.ds(s * BLK, BLK)]
 
-    right, left = a_peer(1), a_peer(nz - 1)
-
     def kv_hop(s, forward, part):
+        source = RELAY[s]
+        way = s - source if forward else nz - s + source
         if part == 2:
-            src, dst = (s - 1, s) if forward else ((nz - s + 1) % nz, nz - s)
-            return rcopy(qbuf.at[src], qbuf.at[dst], q_ss.at[dst], q_rs.at[dst], b_peer(1 if forward else nz - 1))
+            src, dst = (source, s) if forward else ((nz - source) % nz, nz - s)
+            return rcopy(qbuf.at[src], qbuf.at[dst], q_ss.at[dst], q_rs.at[dst], b_peer(way))
         if forward:
-            src, dst, ss, rs, dev = max(2 * s - 3, 0), 2 * s - 1, kf_ss, kf_rs, right
+            src, dst, ss, rs = max(2 * source - 1, 0), 2 * s - 1, kf_ss, kf_rs
         else:
-            src, dst, ss, rs, dev = 2 * s - 2, 2 * s, kb_ss, kb_rs, left
+            src, dst, ss, rs = 2 * source, 2 * s, kb_ss, kb_rs
         at = (k_at, v_at)[part]
-        return rcopy(at(src), at(dst), ss.at[s - 1, part], rs.at[s - 1, part], dev)
-
-    def kv_start(s, parts):
-        for part in parts:
-            if s <= nf:
-                go(kv_hop(s, True, part))
-            if s <= nb:
-                go(kv_hop(s, False, part))
+        return rcopy(at(src), at(dst), ss.at[s - 1, part], rs.at[s - 1, part], a_peer(way))
+
+    def kv_start(source, part, ways=(True, False)):
+        for s in range(nf, 0, -1):
+            if RELAY[s] == source:
+                for forward in ways:
+                    if s <= (nf if forward else nb):
+                        go(kv_hop(s, forward, part))
 
     def kv_advance(s):
         for part in range(3):
-            if s <= nf:
-                kv_hop(s, True, part).wait_recv()
-                if s + 1 <= nf:
-                    go(kv_hop(s + 1, True, part))
-            if s <= nb:
-                kv_hop(s, False, part).wait_recv()
-                if s + 1 <= nb:
-                    go(kv_hop(s + 1, False, part))
-
-    kv_start(1, (0, 1))
+            for forward in (True, False):
+                if s <= (nf if forward else nb):
+                    kv_hop(s, forward, part).wait_recv()
+                    kv_start(s, part, (forward,))
+
+    kv_start(0, 0)
+    kv_start(0, 1)
 
     rest = dot(xs, w[:, 256:768])
     qbuf[0] = (rest[:, 0:128].astype(BF).astype(F32) * (64 ** (-0.5))).T.astype(BF)
-    kv_start(1, (2,))
+    kv_start(0, 2)
 
     rq, rk, rv = (rest[:, 128 * i : 128 * (i + 1)].astype(BF) for i in (1, 2, 3))
     keyed = (rk.astype(F32) * key_weight).T
     state = dot(keyed, rv.astype(F32), precision=HIGH)
-    sa[...] = state.reshape(ny, sl, BLK)
+    sa[...] = state.reshape(ny, sl, BLK).astype(BF)
     ra[pl.ds(y, 1)] = sa[pl.ds(y, 1)]
     rda[pl.ds(y, 1)] = sda[...].reshape(1, 1, BLK)
     for d in range(1, ny):
@@ -284,14 +283,14 @@
         p, dev = y_peer(ny - d)
         rcopy(sa.at[p], ra.at[p], a_ss.at[d, 0], a_rs.at[d, 0], dev).wait_recv()
         rcopy(sda, rda.at[p], a_ss.at[d, 1], a_rs.at[d, 1], dev).wait_recv()
-    total = ra[0]
+    total = ra[0].astype(F32)
     decay = rda[0]
     for i in range(1, ny):
-        total = rda[i] * total + ra[i]
+        total = rda[i] * total + ra[i].astype(F32)
         decay = decay * rda[i]
-    sb[...] = total
+    sb[...] = total.astype(BF)
     sdb[...] = decay
-    rb[pl.ds(z, 1)] = jnp.zeros((1, sl, BLK), F32)
+    rb[pl.ds(z, 1)] = jnp.zeros((1, sl, BLK), BF)
     rdb[pl.ds(z, 1)] = jnp.zeros((1, 1, BLK), F32)
     for d in range(1, nz):
         dev = z_peer(d)[1]
@@ -387,10 +386,10 @@
         rcopy(sdb, rdb.at[p], b_ss.at[d, 1], b_rs.at[d, 1], dev).wait_recv()
     entry = init[0, pl.ds(pl.multiple_of(y * sl, sl), sl), :].astype(F32)
     for i in range(nz):
-        entry = jnp.where(i < z, rdb[i] * entry + rb[i], entry)
+        entry = jnp.where(i < z, rdb[i] * entry + rb[i].astype(F32), entry)
     for i in range(ny):
-        sc[i] = entry
-        entry = rda[i] * entry + ra[i]
+        sc[i] = entry.astype(BF)
+        entry = rda[i] * entry + ra[i].astype(F32)
     rc[pl.ds(y, 1)] = sc[pl.ds(y, 1)]
     for d in range(1, ny):
         p, dev = y_peer(d)
@@ -413,7 +412,7 @@
     for d in range(1, ny):
         p, dev = y_peer(ny - d)
         rcopy(sc.at[p], rc.at[p], c_ss.at[d], c_rs.at[d], dev).wait_recv()
-    ret = inner + dot(reaching, rc[...].reshape(BLK, BLK), precision=HIGH)
+    ret = inner + dot(reaching, rc[...].reshape(BLK, BLK).astype(F32), precision=HIGH)
     centre = ret - jnp.mean(ret, axis=-1, keepdims=True)
     ret_mix = (
         centre * lax.rsqrt(jnp.mean(centre * centre, axis=-1, keepdims=True) + EPS) * rgain[...]
@@ -446,7 +445,7 @@
         mine = mixb[:, pl.ds(c, 1)].reshape(nx * rows, 256)
         mix = jnp.concatenate([mine, pmix[...].reshape(nx * rows, 256)], axis=1)
     fs[...] = dot(mix, wpair[...]).astype(BF).reshape(nx, rows, width)
-    for d in range(1, nx):
+    for d in far_first:
         p, dev = x_peer(d)
         go(rcopy(fs.at[p], fr.at[d], f_ss.at[d], f_rs.at[d], dev))
     acc = fs[pl.ds(fx, 1)].reshape(rows, width).astype(F32)
@@ -484,9 +483,9 @@
         vm((1, BLK), F32), vm((1, BLK), F32), vm((2, BLK, width), BF), vm((width, 768), BF), vm((BLK, width), BF),
         vm((nz * BLK, BLK), BF), vm((BLK, nz * BLK), BF), vm((ny, BLK, BLK), BF),
         vm((ny, BLK, 2 * BLK), BF), vm((ny, 2, 2 * BLK), F32), vm((ny, BLK, 2 * BLK), BF), vm((ny, 2, 2 * BLK), F32),
-        vm((ny, sl, BLK), F32), vm((1, BLK), F32), vm((ny, sl, BLK), F32), vm((ny, 1, BLK), F32),
-        vm((sl, BLK), F32), vm((1, BLK), F32), vm((nz, sl, BLK), F32), vm((nz, 1, BLK), F32),
-        vm((ny, sl, BLK), F32), vm((ny, sl, BLK), F32),
+        vm((ny, sl, BLK), BF), vm((1, BLK), F32), vm((ny, sl, BLK), BF), vm((ny, 1, BLK), F32),
+        vm((sl, BLK), BF), vm((1, BLK), F32), vm((nz, sl, BLK), BF), vm((nz, 1, BLK), F32),
+        vm((ny, sl, BLK), BF), vm((ny, sl, BLK), BF),
         vm((nz // 2, BLK, 4 * BLK), F32), vm((nz // 2, 2, 4 * BLK), F32),
         vm((2, nz, ny, 32, BLK), BF), vm((2, nz, ny, 32, BLK), BF), vm((2 * nc * BLK, width), BF),
         vm((nx, nc, rows, 2 * BLK), BF), vm((nx, rows, 2 * BLK), BF), vm((nx, rows, width), BF), vm((nx, rows, width), BF),

time: 59.5 us -> 58.4 us (0.982)
  Pallas kernels: 57.2 us -> 56.1 us
    pallas_call x1, Pallas kernels: 57.2 us -> 56.1 us  [local(): pl.pallas_call(functools.partial(kernel, dims), out_shape=jax.ShapeDtypeS...]
where the time goes in v4:
time: 58.4 us; the launch traced here: 58.2 us
  Pallas kernels  56.1 us (96%)
  local copies, waits for them, and re-layouts  1.47 us (3%)
  between operations  0.66 us (1%)
    pallas_call x1, Pallas kernels, local(): pl.pallas_call(functools.partial(kernel, dims), out_shape=jax.ShapeDtypeS...  56.1 us
    unnamed x1, local copies, waits for them, and re-layouts  1.47 us

profile of v4, /device:TPU:1, one launch (start us, length us, event | category | flops | bytes accessed | tf_op | source)
XLA Modules:
  0.0 58.2 jit_solution(16038565724691233459)
XLA Ops:
  0.7 56.1 %shard_map.136 = bf16[16,2048]{1,0:T(8,128)(2,1)} custom-call(bf16[16,2048]{1,0:T(8,128)(2,1)} %tok_h.1, f32[1,2048]{1,0:T(1,128)} %bitcast.13, bf16[2048,128]{1,0:T(8,128)(2,1)} %wrq_h.1, bf16[2048,128]{1,0:T(8,128)(2,1)} %wrk_h.1, bf16[2048,128]{1,0:T(8,128)(2,1)} %wrv_h.1, f32[1,128]{1,0:T(1,128)} %dec_h.1, bf16[1,128,128]{2,1,0:T(8,128)(2,1)} %init_h.1, ...), custom_call_target="tpu_custom_call" | custom-call | tf_op jit(solution)/shard_map/pallas_call | solution.py:500
  56.8 1.5 %copy.17 = bf16[16,2048]{1,0:T(8,128)(2,1)} copy(bf16[16,2048]{1,0:T(8,128)(2,1)} %shard_map.136) | data formatting | bytes 131072

commit v5 on v4

--- a/solution.py
+++ b/solution.py
@@ -115,7 +115,6 @@
     scale = lax.rsqrt(jnp.mean(t * t, axis=-1, keepdims=True) + EPS)
     own_x = x.at[pl.ds(pl.multiple_of(h * rows, rows), rows), :]
     own_x[...] = (t * scale * gain[...]).astype(BF)
-    loads[2].wait()
 
     pl.semaphore_wait(barrier, nh + ny + nz - 3)
 
@@ -133,6 +132,7 @@
         go(rcopy(own_x, own_x, tok_ss.at[d], tok_rs.at[d], x_peer(d)[1]))
     if nc > 1:
         go(rcopy(own_x, own_x, pt_ss.at[0], pt_rs.at[0], partner))
+    loads[2].wait()
     for d in range(1, ny):
         part = wt.at[0, z, y]
         go(rcopy(part, part, ow_ss.at[d, 0], ow_rs.at[d, 0], y_peer(d)[1]))
@@ -305,7 +305,7 @@
     top_half = row < 64
 
     def pair(i):
-        return nz // 2 - i, lax.rem(nz // 2 + 1 + i, nz)
+        return nz // 2 - i, (nz // 2 + 1 + i) % nz
 
     def attend(i, lo, hi):
         places, wide = [], []
@@ -339,20 +339,19 @@
         sums = dot(vtall[:, lo * BLK : hi * BLK], jnp.concatenate(probs, axis=1))
         return sums, jnp.concatenate(peaks, axis=1), jnp.concatenate(totals, axis=1), places
 
-    def attend_early(near, _):
-        i = nz // 2 - 1 - near
-        sums, peak, total, _ = attend(i, 0, early)
-        early_sum[pl.ds(i, 1)] = sums[None]
-        early_stat[pl.ds(i, 1)] = jnp.concatenate([peak, total], axis=0)[None]
-        return 0
-
-    def attend_late(i, _):
+    def absorb(i, lo, hi):
         first, second = pair(i)
-        sums, peak, total, places = attend(i, early, nz)
-        share = jnp.exp(early_stat[i, 0:1, :] - peak)
-        total = total + share * early_stat[i, 1:2, :]
-        sums = (sums + share * early_sum[i]).astype(BF)
+        sums, peak, total, places = attend(i, lo, hi)
+        if lo:
+            share = jnp.exp(early_stat[i, 0:1, :] - peak)
+            total = total + share * early_stat[i, 1:2, :]
+            sums = sums + share * early_sum[i]
         stat = jnp.concatenate([peak, total], axis=0)
+        if hi < nz:
+            early_sum[i] = sums
+            early_stat[i] = stat
+            return
+        sums = sums.astype(BF)
         so[pl.ds(first, 1)] = sums[None, :, 0:256]
         so[pl.ds(second, 1)] = sums[None, :, 256:512]
         st[pl.ds(first, 1)] = stat[None, :, 0:256]
@@ -365,20 +364,24 @@
 
         send(first, places[0])
 
-        @pl.when(i < nz // 2 - 1)
-        def _():
+        if second:
             send(second, places[1])
 
-        return 0
-
     pairs = nz // 2
-    lax.fori_loop(0, min(2, pairs), attend_early, 0)
-    for s in range(3, nf + 1):
-        ow_wait(s - 1)
-        ow_start(s)
-        ow_pass(s - 1)
-        kv_advance(s)
-        lax.fori_loop(s - 1, s, attend_early, 0)
+    middle = nz - 1 if nf > 2 else early
+    absorb(pairs - 1, 0, early)
+    if nf > 2:
+        absorb(pairs - 2, 0, early)
+        ow_wait(2)
+        ow_start(3)
+        ow_pass(2)
+        kv_advance(3)
+        absorb(pairs - 3, 0, middle)
+        ow_wait(3)
+        ow_start(4)
+        ow_pass(3)
+        absorb(pairs - 1, early, middle)
+        absorb(pairs - 2, early, middle)
 
     for d in range(1, nz):
         p, dev = z_peer(nz - d)
@@ -395,7 +398,11 @@
         p, dev = y_peer(d)
         rcopy(sc.at[p], rc.at[y], c_ss.at[d], c_rs.at[d], dev).start()
 
-    lax.fori_loop(0, pairs, attend_late, 0)
+    if nf > 2:
+        kv_advance(4)
+    absorb(0, 0, nz)
+    for i in range(1, pairs):
+        absorb(i, middle, nz)
 
     width = out_ref.shape[1]
     ow_wait(nf)

time: 58.4 us -> 58.1 us (level)
  no operation moved by 1% of the time
where the time goes in v5:
time: 58.1 us; the launch traced here: 57.9 us
  Pallas kernels  55.8 us (96%)
  local copies, waits for them, and re-layouts  1.47 us (3%)
  between operations  0.66 us (1%)
    pallas_call x1, Pallas kernels, local(): pl.pallas_call(functools.partial(kernel, dims), out_shape=jax.ShapeDtypeS...  55.8 us
    unnamed x1, local copies, waits for them, and re-layouts  1.47 us

profile of v5, /device:TPU:1, one launch (start us, length us, event | category | flops | bytes accessed | tf_op | source)
XLA Modules:
  0.0 57.9 jit_solution(13031760998320446970)
XLA Ops:
  0.7 55.8 %shard_map.136 = bf16[16,2048]{1,0:T(8,128)(2,1)} custom-call(bf16[16,2048]{1,0:T(8,128)(2,1)} %tok_h.1, f32[1,2048]{1,0:T(1,128)} %bitcast.13, bf16[2048,128]{1,0:T(8,128)(2,1)} %wrq_h.1, bf16[2048,128]{1,0:T(8,128)(2,1)} %wrk_h.1, bf16[2048,128]{1,0:T(8,128)(2,1)} %wrv_h.1, f32[1,128]{1,0:T(1,128)} %dec_h.1, bf16[1,128,128]{2,1,0:T(8,128)(2,1)} %init_h.1, ...), custom_call_target="tpu_custom_call" | custom-call | tf_op jit(solution)/shard_map/pallas_call | solution.py:507
  56.4 1.5 %copy.17 = bf16[16,2048]{1,0:T(8,128)(2,1)} copy(bf16[16,2048]{1,0:T(8,128)(2,1)} %shard_map.136) | data formatting | bytes 131072
